TPU v7x, 256 devices: a whole 4x4x8 slice. The times are simulated.
256 devices in a mesh: sp: 32 (over z, x), tp: 8 (over y, core).
Axes of the slice: x: 4, y: 4, z: 8, core: 2. Of those that a mesh axis runs over, the one named last changes fastest.
Arguments:
- tokens: bfloat16 [8192, 4096], P('sp', 'tp'), may hold values from -6 to 6
- norm_gain: float32 [4096], replicated, may hold values from 0.1 to 1.9
- fox_query: bfloat16 [4096, 1024], P(None, 'tp'), may hold values from -0.234375 to 0.234375
- fox_key: bfloat16 [4096, 1024], P(None, 'tp'), may hold values from -0.09375 to 0.09375
- fox_value: bfloat16 [4096, 1024], P(None, 'tp'), may hold values from -0.09375 to 0.09375
- cum_gate: float32 [8, 8192], P('tp'), as said below
- lin_query: bfloat16 [4096, 1024], P(None, 'tp'), may hold values from -0.09375 to 0.09375
- lin_key: bfloat16 [4096, 1024], P(None, 'tp'), may hold values from -0.09375 to 0.09375
- lin_value: bfloat16 [4096, 2048], P(None, 'tp'), may hold values from -0.09375 to 0.09375
- decay_down: bfloat16 [4096, 16], replicated, may hold values from -0.09375 to 0.09375
- decay_up: bfloat16 [16, 1024], P(None, 'tp'), may hold values from -1.5 to 1.5
- decay_bias: float32 [1024], P('tp'), may hold values from 0.5 to 11
- lin_gain: float32 [256], replicated, may hold values from 0.1 to 1.9
- fox_out: bfloat16 [1024, 4096], P('tp'), may hold values from -0.109375 to 0.109375
- lin_out: bfloat16 [2048, 4096], P('tp'), may hold values from -0.109375 to 0.109375
Outputs:
- mixed: bfloat16 [8192, 4096], P(('sp', 'tp'))
- log_total: float32 [8, 8192], P('tp', 'sp')
Inputs may be any that keep to these rules, and one draw needn't show every extreme that they name: `cum_gate`: along positions each head's values never rise.
All inputs are finite; a program needn't handle non-finite values.
Results may differ from a plain program's by a relative error of at most 0.017.
Values may be sent and summed in bfloat16 or wider, within the bound.
A program may use at most 64 MiB of HBM per device.

v0:
```python
import math

import jax
import jax.numpy as jnp
from jax import lax
from jax.sharding import Mesh
from jax.sharding import PartitionSpec as P

HEAD = 128
KEY_DIM = 128
VAL_DIM = 256
BLOCK = 64
SP = ("sp_0", "sp_1")
SP_TP = ("sp_0", "sp_1", "tp")


EPS = 1e-06
TAU = 16.0


def from_everyone(array, axis):
    size = lax.axis_size(axis)
    return lax.all_to_all(
        jnp.broadcast_to(array[None], (size, *array.shape)), axis, 0, 0, tiled=True
    )


def joined_along(blocks, dim):
    blocks = jnp.moveaxis(blocks, 0, dim)
    lengths = blocks.shape
    return blocks.reshape(*lengths[:dim], lengths[dim] * lengths[dim + 1], *lengths[dim + 2 :])


def collect(array, axis, dim):
    blocks = from_everyone(array, axis)
    return joined_along(blocks, dim)


def sent_together(arrays, axis, dim, along):
    widths = [a.shape[along] for a in arrays]
    both = jnp.concatenate(arrays, axis=along)
    whole = lax.all_gather(both, axis, axis=dim, tiled=True)
    return tuple(jnp.split(whole, [sum(widths[:k]) for k in range(1, len(widths))], axis=along))


def neutral_like(array, identity):
    return jax.tree.map(
        lambda part, zero: jnp.zeros_like(part) + jnp.asarray(zero, part.dtype), array, identity
    )


def carried_in(array, axes, combine, identity):
    before = start = neutral_like(array, identity)
    total = array
    for axis in reversed(axes):
        size, index = (lax.axis_size(axis), lax.axis_index(axis))
        pieces = jax.tree.map(
            lambda part, kind: lax.all_gather(part.astype(kind), axis),
            total,
            (jnp.bfloat16, jnp.bfloat16),
        )
        inside, total = (start, start)
        for k in range(size):
            passed = k < index
            total = combine(
                total, jax.tree.map(lambda part, own: part[k].astype(own.dtype), pieces, array)
            )
            inside = jax.tree.map(lambda new, old: jnp.where(passed, new, old), total, inside)
        before = combine(inside, before)
    return before


def cut_along(array, dim, size):
    lengths = array.shape
    blocks = array.reshape(*lengths[:dim], size, lengths[dim] // size, *lengths[dim + 1 :])
    return jnp.moveaxis(blocks, dim, 0)


def summed_on_arrival(array, axis, dim):
    blocks = cut_along(array, dim, lax.axis_size(axis))
    arrived = lax.all_to_all(blocks, axis, split_axis=0, concat_axis=0, tiled=True)
    return arrived.astype(jnp.float32).sum(axis=0)


def rms_scale(values, gain):
    return values * lax.rsqrt(jnp.mean(values * values, axis=-1, keepdims=True) + EPS) * gain


def block_step(state, q_b, k_b, v_b, cum):
    inter = jnp.dot(q_b * jnp.exp(cum), state)
    span = cum.shape[0]
    causal = jnp.arange(span)[:, None] >= jnp.arange(span)[None, :]
    rel = cum[:, None, :] - cum[None, :, :]
    decay = jnp.exp(jnp.where(causal[:, :, None], rel, -jnp.inf))
    scores = jnp.einsum("id,jd,ijd->ij", q_b, k_b, decay)
    intra = jnp.dot(scores, v_b)
    last = cum[-1]
    new_state = jnp.exp(last)[:, None] * state + jnp.dot(
        (k_b * jnp.exp(last[None, :] - cum)).T, v_b
    )
    return (new_state, inter + intra)


def local_pass(q, k, v, g):
    count = q.shape[0] // BLOCK

    def step(carry, item):
        state, run = carry
        q_b, k_b, v_b, g_b = item
        cum = jnp.cumsum(g_b, axis=0)
        new_state, out = block_step(state, q_b, k_b, v_b, cum)
        attention_extent = q_b * jnp.exp(run[None, :] + cum)
        return ((new_state, run + cum[-1]), (out, attention_extent))

    items = (
        q.reshape(count, BLOCK, KEY_DIM),
        k.reshape(count, BLOCK, KEY_DIM),
        v.reshape(count, BLOCK, VAL_DIM),
        g.reshape(count, BLOCK, KEY_DIM),
    )
    start = (jnp.zeros((KEY_DIM, VAL_DIM), jnp.float32), jnp.zeros((KEY_DIM,), jnp.float32))
    (state, run), (out, attention_extent) = lax.scan(step, start, items)
    return (out.reshape(-1, VAL_DIM), attention_extent.reshape(-1, KEY_DIM), state, run)


def local(
    tokens,
    norm_gain,
    fox_query,
    fox_key,
    fox_value,
    cum_gate,
    lin_query,
    lin_key,
    lin_value,
    decay_down,
    decay_up,
    decay_bias,
    lin_gain,
    fox_out,
    lin_out,
):
    whole = collect(tokens, "tp", 1)
    normed = rms_scale(whole.astype(jnp.float32), norm_gain).astype(jnp.bfloat16)
    tok_rows = normed.shape[0]
    offset = lax.axis_index(SP) * tok_rows

    def project(weight):
        return jnp.dot(normed, weight, preferred_element_type=jnp.float32).astype(jnp.bfloat16)

    fox_here = fox_query.shape[1] // HEAD
    queries = project(fox_query).reshape(tok_rows, fox_here, HEAD)
    keys_here = project(fox_key)
    values_here = project(fox_value)
    q_cum = lax.dynamic_slice_in_dim(cum_gate, offset, tok_rows, 1)
    q_pos = offset + jnp.arange(tok_rows, dtype=jnp.int32)
    scale = HEAD ** (-0.5)
    begin = (
        jnp.full((fox_here, tok_rows), -jnp.inf, jnp.float32),
        jnp.zeros((fox_here, tok_rows), jnp.float32),
        jnp.zeros((fox_here, tok_rows, HEAD), jnp.float32),
    )
    carry = begin
    key_rows, value_rows = sent_together((keys_here, values_here), SP, 0, 1)
    span = key_rows.shape[0]
    sub = math.gcd(span, 512)
    key_blocks = key_rows.reshape(span // sub, sub, fox_here, HEAD)
    value_blocks = value_rows.reshape(span // sub, sub, fox_here, HEAD)

    def inner(state, item):
        key_blk, value_blk, index = item
        first = index * sub

        def work(current):
            top, total, acc = current
            k_cum = lax.dynamic_slice_in_dim(cum_gate, first, sub, 1)
            logits = (
                jnp.einsum("qhd,khd->hqk", queries, key_blk, preferred_element_type=jnp.float32)
                * scale
            )
            logits = logits + q_cum[:, :, None] - k_cum[:, None, :]
            k_pos = first + jnp.arange(sub, dtype=jnp.int32)
            logits = jnp.where(k_pos[None, None, :] <= q_pos[None, :, None], logits, -jnp.inf)
            new_top = jnp.maximum(top, jnp.max(logits, axis=2))
            safe = jnp.where(new_top == -jnp.inf, 0.0, new_top)
            weights = jnp.exp(logits - safe[:, :, None])
            shrink = jnp.exp(top - safe)
            new_total = total * shrink + jnp.sum(weights, axis=2)
            new_acc = acc * shrink[:, :, None] + jnp.einsum(
                "hqk,khd->hqd",
                weights.astype(jnp.bfloat16),
                value_blk,
                preferred_element_type=jnp.float32,
            )
            return (new_top, new_total, new_acc)

        return (lax.cond(first < offset + tok_rows, work, lambda current: current, state), None)

    carry, _ = lax.scan(
        inner, carry, (key_blocks, value_blocks, jnp.arange(span // sub, dtype=jnp.int32))
    )
    top, total, acc = carry
    log_total = top + jnp.log(total)
    fox_flat = (
        (acc / total[:, :, None])
        .astype(jnp.bfloat16)
        .transpose(1, 0, 2)
        .reshape(tok_rows, fox_here * HEAD)
    )
    lin_here = lin_query.shape[1] // KEY_DIM
    lq = project(lin_query).astype(jnp.float32) * KEY_DIM ** (-0.5)
    lk = project(lin_key).astype(jnp.float32)
    lv = project(lin_value).astype(jnp.float32)
    low = project(decay_down)
    log_decay = (
        jax.nn.log_sigmoid(jnp.dot(low, decay_up, preferred_element_type=jnp.float32) + decay_bias)
        / TAU
    )

    def by_head(values, width):
        return values.reshape(tok_rows, lin_here, width).transpose(1, 0, 2)

    local_out, attention_extent, states, totals = jax.vmap(local_pass)(
        by_head(lq, KEY_DIM),
        by_head(lk, KEY_DIM),
        by_head(lv, VAL_DIM),
        by_head(log_decay, KEY_DIM),
    )

    def combine(earlier, later):
        return (earlier[0] + later[0], jnp.exp(later[0])[..., None] * earlier[1] + later[1])

    identity = (jnp.zeros_like(totals), jnp.zeros_like(states))
    _, passed_forward = carried_in((totals, states), SP, combine, identity)
    lin_raw = local_out + jnp.einsum("ejg,egc->ejc", attention_extent, passed_forward)
    lin_heads = rms_scale(lin_raw, lin_gain).astype(jnp.bfloat16)
    lin_flat = lin_heads.transpose(1, 0, 2).reshape(tok_rows, lin_here * VAL_DIM)
    term = jnp.dot(fox_flat, fox_out, preferred_element_type=jnp.float32)
    mixed = summed_on_arrival(
        (term + jnp.dot(lin_flat, lin_out, preferred_element_type=jnp.float32)).astype(
            jnp.bfloat16
        ),
        "tp",
        0,
    ).astype(jnp.bfloat16)
    return (mixed, log_total)


def solution(mesh):
    torus = Mesh(mesh.devices.reshape(8, 4, mesh.shape["tp"]), ("sp_0", "sp_1", "tp"))
    in_specs = (
        P(SP, "tp"),
        P(),
        P(None, "tp"),
        P(None, "tp"),
        P(None, "tp"),
        P("tp", None),
        P(None, "tp"),
        P(None, "tp"),
        P(None, "tp"),
        P(),
        P(None, "tp"),
        P("tp"),
        P(),
        P("tp", None),
        P("tp", None),
    )
    out_specs = (P(SP_TP, None), P("tp", SP))
    return jax.shard_map(local, mesh=torus, in_specs=in_specs, out_specs=out_specs, check_vma=False)
```

profile of v0, /device:TPU:224, one launch (start us, length us, event | category | flops | bytes accessed | tf_op | source)
XLA Modules:
  0.0 277.7 jit_solution(16357137265273203041)
XLA Ops:
  7.2 1.2 copy.45
  8.4 1.5 broadcast_in_dim.45
  9.9 4.5 %all-to-all-start = ((bf16[8,256,512]{1,2,0:T(8,128)(2,1)}), bf16[8,256,512]{1,2,0:T(8,128)(2,1)}, u32[]{:S(2)}, u32[]{:S(2)}) async-start(bf16[8,256,512]{1,2,0:T(8,128)(2,1)} %broadcast_in_dim.45), calls=%async_computation | async-start | bytes 4194304 | tf_op jit(solution)/shard_map/all_to_all | solution.py:23
  14.5 1.2 constant_dynamic-slice_fusion.1
  15.7 25.9 %all-to-all-done = bf16[8,256,512]{1,2,0:T(8,128)(2,1)} async-done(((bf16[8,256,512]{1,2,0:T(8,128)(2,1)}), bf16[8,256,512]{1,2,0:T(8,128)(2,1)}, u32[]{:S(2)}, u32[]{:S(2)}) %all-to-all-start) | async-done | bytes 2097184 | tf_op jit(solution)/shard_map/all_to_all | solution.py:23
  41.6 2.2 multiply_reduce_fusion
  43.8 2.0 fusion.52
  46.4 1.4 copy-done.15
  49.2 2.5 convolution_convert_fusion.2
  54.2 2.3 fusion.79
  56.4 14.8 %while.35 = (s32[]{:T(128)}, f32[1,128,256]{2,1,0:T(8,128)S(1)}, f32[1,128]{1,0:T(1,128)S(1)}, f32[4,1,64,256]{3,2,1,0:T(8,128)S(1)}, bf16[4,1,64,128]{3,2,1,0:T...) while((s32[]{:T(128)}, f32[1,128,256]{2,1,0:T(8,128)S(1)}, ...), condition=%wide.region_9.10_spmd.clone, body=%wide.region_7.9_spmd.clone.sunk | while | flops 13811971 | bytes 5447825 | solution.py:122
  57.9 1.7 fusion.205
  61.5 1.7 fusion.205
  65.2 1.7 fusion.205
  68.9 1.7 fusion.205
  72.1 9.8 %all-gather.2 = bf16[4,1,128]{2,1,0:T(2,128)(2,1)S(1)} all-gather(bf16[1,1,128]{2,1,0:T(2,128)(2,1)S(1)} %convert_bitcast_fusion.9), channel_id=2, replica_groups=mesh['sp_0'=8,'sp_1'=4,'tp'=8] {'sp_1'}, dimensions={0}, use_global_device_ids=true | all-gather | bytes 1280 | tf_op jit(solution)/shard_map/all_gather | solution.py:58
  82.0 13.1 %all_gather.26 = bf16[8,1,128]{2,1,0:T(2,128)(2,1)S(1)} all-gather(bf16[1,1,128]{2,1,0:T(2,128)(2,1)S(1)} %get-tuple-element.509), channel_id=1, replica_groups=mesh['sp_0'=8,'sp_1'=4,'tp'=8] {'sp_0'}, dimensions={0}, use_global_device_ids=true | all-gather | bytes 2304 | tf_op jit(solution)/shard_map/all_gather | solution.py:58
  95.1 13.0 %all-gather.1 = bf16[4,128,256]{2,1,0:T(8,128)(2,1)S(1)} all-gather(bf16[1,128,256]{2,1,0:T(8,128)(2,1)S(1)} %convert_element_type.535), channel_id=3, replica_groups=mesh['sp_0'=8,'sp_1'=4,'tp'=8] {'sp_1'}, dimensions={0}, use_global_device_ids=true | all-gather | bytes 327680 | tf_op jit(solution)/shard_map/all_gather | solution.py:58
  108.3 26.9 %all_gather.29 = bf16[8,1,128,256]{3,2,1,0:T(8,128)(2,1)S(1)} all-gather(bf16[1,1,128,256]{3,2,1,0:T(8,128)(2,1)S(1)} %fusion.64), channel_id=1, replica_groups=mesh['sp_0'=8,'sp_1'=4,'tp'=8] {'sp_0'}, dimensions={0}, use_global_device_ids=true | all-gather | bytes 589824 | tf_op jit(solution)/shard_map/all_gather | solution.py:58
  135.1 1.6 multiply_reduce_fusion.1
  136.8 1.4 fusion.56
  138.2 4.6 %fusion.161 = (bf16[8192,128]{0,1:T(8,128)(2,1)}, bf16[8192,128]{0,1:T(8,128)(2,1)}) fusion(bf16[8192,256]{0,1:T(8,128)(2,1)} %all-gather.5.cloned.1.call-done), kind=kLoop, calls=%fused_computation.242 | loop fusion | bytes 8388608 | tf_op jit(solution)/shard_map/split | solution.py:43
  142.8 4.1 %copy.60 = bf16[8192,128]{1,0:T(8,128)(2,1)} copy(bf16[8192,128]{0,1:T(8,128)(2,1)} %get-tuple-element.499) | data formatting | bytes 4194304
  146.9 4.1 %copy.61 = bf16[8192,128]{1,0:T(8,128)(2,1)} copy(bf16[8192,128]{0,1:T(8,128)(2,1)} %get-tuple-element.498) | data formatting | bytes 4194304
  151.5 82.1 %while.34 = (s32[]{:T(128)}, f32[1,256]{1,0:T(1,128)S(1)}, f32[1,256]{1,0:T(1,128)S(1)}, f32[1,256,128]{2,1,0:T(8,128)S(1)}, s32[16]{0:T(128)}, /*index=5*/s32[]...) while((s32[]{:T(128)}, f32[1,256]{1,0:T(1,128)S(1)}, ...), condition=%wide.region_6.7_spmd.clone, body=%wide.region_1.6_spmd.clone.sunk | while | flops 68487424 | bytes 2196849 | solution.py:199
  151.6 1.3 dynamic_slice.93
  153.5 3.4 %conditional.3 = ((f32[1,256]{1,0:T(1,128)S(1)}, f32[1,256]{1,0:T(1,128)S(1)}, f32[1,256,128]{2,1,0:T(8,128)S(1)})) conditional(s32[]{:T(128)} %convert_element_type.773, (f32[1,256]{1,0:T(1,128)S(1)}, f32[1,256]{1,0:T(1,128)S(1)}, f32[1,256,128]{2,1,0:T(8,128)S(1)}) %tuple.92, (s32[]{:T(128)}, s32[]{:T(128)}, bf16[16,512,1,128]{3,1,2,0:T(8,128)(2,1)}, ...), branch_computations={%region_2.2_spmd, %region_3.5_spmd} | conditional | flops 68487424 | bytes 2195534 | solution.py:197
  157.0 1.3 dynamic_slice.93
  158.9 3.4 %conditional.3 = ((f32[1,256]{1,0:T(1,128)S(1)}, f32[1,256]{1,0:T(1,128)S(1)}, f32[1,256,128]{2,1,0:T(8,128)S(1)})) conditional(s32[]{:T(128)} %convert_element_type.773, (f32[1,256]{1,0:T(1,128)S(1)}, f32[1,256]{1,0:T(1,128)S(1)}, f32[1,256,128]{2,1,0:T(8,128)S(1)}) %tuple.92, (s32[]{:T(128)}, s32[]{:T(128)}, bf16[16,512,1,128]{3,1,2,0:T(8,128)(2,1)}, ...), branch_computations={%region_2.2_spmd, %region_3.5_spmd} | conditional | flops 68487424 | bytes 2195534 | solution.py:197
  162.3 1.3 dynamic_slice.93
  164.2 3.4 %conditional.3 = ((f32[1,256]{1,0:T(1,128)S(1)}, f32[1,256]{1,0:T(1,128)S(1)}, f32[1,256,128]{2,1,0:T(8,128)S(1)})) conditional(s32[]{:T(128)} %convert_element_type.773, (f32[1,256]{1,0:T(1,128)S(1)}, f32[1,256]{1,0:T(1,128)S(1)}, f32[1,256,128]{2,1,0:T(8,128)S(1)}) %tuple.92, (s32[]{:T(128)}, s32[]{:T(128)}, bf16[16,512,1,128]{3,1,2,0:T(8,128)(2,1)}, ...), branch_computations={%region_2.2_spmd, %region_3.5_spmd} | conditional | flops 68487424 | bytes 2195534 | solution.py:197
  165.0 1.2 fusion.160
  167.6 1.3 dynamic_slice.93
  169.6 3.4 %conditional.3 = ((f32[1,256]{1,0:T(1,128)S(1)}, f32[1,256]{1,0:T(1,128)S(1)}, f32[1,256,128]{2,1,0:T(8,128)S(1)})) conditional(s32[]{:T(128)} %convert_element_type.773, (f32[1,256]{1,0:T(1,128)S(1)}, f32[1,256]{1,0:T(1,128)S(1)}, f32[1,256,128]{2,1,0:T(8,128)S(1)}) %tuple.92, (s32[]{:T(128)}, s32[]{:T(128)}, bf16[16,512,1,128]{3,1,2,0:T(8,128)(2,1)}, ...), branch_computations={%region_2.2_spmd, %region_3.5_spmd} | conditional | flops 68487424 | bytes 2195534 | solution.py:197
  173.0 1.3 dynamic_slice.93
  174.9 3.4 %conditional.3 = ((f32[1,256]{1,0:T(1,128)S(1)}, f32[1,256]{1,0:T(1,128)S(1)}, f32[1,256,128]{2,1,0:T(8,128)S(1)})) conditional(s32[]{:T(128)} %convert_element_type.773, (f32[1,256]{1,0:T(1,128)S(1)}, f32[1,256]{1,0:T(1,128)S(1)}, f32[1,256,128]{2,1,0:T(8,128)S(1)}) %tuple.92, (s32[]{:T(128)}, s32[]{:T(128)}, bf16[16,512,1,128]{3,1,2,0:T(8,128)(2,1)}, ...), branch_computations={%region_2.2_spmd, %region_3.5_spmd} | conditional | flops 68487424 | bytes 2195534 | solution.py:197
  178.3 1.3 dynamic_slice.93
  180.2 3.4 %conditional.3 = ((f32[1,256]{1,0:T(1,128)S(1)}, f32[1,256]{1,0:T(1,128)S(1)}, f32[1,256,128]{2,1,0:T(8,128)S(1)})) conditional(s32[]{:T(128)} %convert_element_type.773, (f32[1,256]{1,0:T(1,128)S(1)}, f32[1,256]{1,0:T(1,128)S(1)}, f32[1,256,128]{2,1,0:T(8,128)S(1)}) %tuple.92, (s32[]{:T(128)}, s32[]{:T(128)}, bf16[16,512,1,128]{3,1,2,0:T(8,128)(2,1)}, ...), branch_computations={%region_2.2_spmd, %region_3.5_spmd} | conditional | flops 68487424 | bytes 2195534 | solution.py:197
  183.7 1.3 dynamic_slice.93
  185.6 3.4 %conditional.3 = ((f32[1,256]{1,0:T(1,128)S(1)}, f32[1,256]{1,0:T(1,128)S(1)}, f32[1,256,128]{2,1,0:T(8,128)S(1)})) conditional(s32[]{:T(128)} %convert_element_type.773, (f32[1,256]{1,0:T(1,128)S(1)}, f32[1,256]{1,0:T(1,128)S(1)}, f32[1,256,128]{2,1,0:T(8,128)S(1)}) %tuple.92, (s32[]{:T(128)}, s32[]{:T(128)}, bf16[16,512,1,128]{3,1,2,0:T(8,128)(2,1)}, ...), branch_computations={%region_2.2_spmd, %region_3.5_spmd} | conditional | flops 68487424 | bytes 2195534 | solution.py:197
  186.4 1.2 fusion.160
  189.0 1.3 dynamic_slice.93
  190.9 3.4 %conditional.3 = ((f32[1,256]{1,0:T(1,128)S(1)}, f32[1,256]{1,0:T(1,128)S(1)}, f32[1,256,128]{2,1,0:T(8,128)S(1)})) conditional(s32[]{:T(128)} %convert_element_type.773, (f32[1,256]{1,0:T(1,128)S(1)}, f32[1,256]{1,0:T(1,128)S(1)}, f32[1,256,128]{2,1,0:T(8,128)S(1)}) %tuple.92, (s32[]{:T(128)}, s32[]{:T(128)}, bf16[16,512,1,128]{3,1,2,0:T(8,128)(2,1)}, ...), branch_computations={%region_2.2_spmd, %region_3.5_spmd} | conditional | flops 68487424 | bytes 2195534 | solution.py:197
  194.3 1.3 dynamic_slice.93
  196.2 3.4 %conditional.3 = ((f32[1,256]{1,0:T(1,128)S(1)}, f32[1,256]{1,0:T(1,128)S(1)}, f32[1,256,128]{2,1,0:T(8,128)S(1)})) conditional(s32[]{:T(128)} %convert_element_type.773, (f32[1,256]{1,0:T(1,128)S(1)}, f32[1,256]{1,0:T(1,128)S(1)}, f32[1,256,128]{2,1,0:T(8,128)S(1)}) %tuple.92, (s32[]{:T(128)}, s32[]{:T(128)}, bf16[16,512,1,128]{3,1,2,0:T(8,128)(2,1)}, ...), branch_computations={%region_2.2_spmd, %region_3.5_spmd} | conditional | flops 68487424 | bytes 2195534 | solution.py:197
  199.7 1.3 dynamic_slice.93
  201.6 3.4 %conditional.3 = ((f32[1,256]{1,0:T(1,128)S(1)}, f32[1,256]{1,0:T(1,128)S(1)}, f32[1,256,128]{2,1,0:T(8,128)S(1)})) conditional(s32[]{:T(128)} %convert_element_type.773, (f32[1,256]{1,0:T(1,128)S(1)}, f32[1,256]{1,0:T(1,128)S(1)}, f32[1,256,128]{2,1,0:T(8,128)S(1)}) %tuple.92, (s32[]{:T(128)}, s32[]{:T(128)}, bf16[16,512,1,128]{3,1,2,0:T(8,128)(2,1)}, ...), branch_computations={%region_2.2_spmd, %region_3.5_spmd} | conditional | flops 68487424 | bytes 2195534 | solution.py:197
  205.0 1.3 dynamic_slice.93
  206.9 3.4 %conditional.3 = ((f32[1,256]{1,0:T(1,128)S(1)}, f32[1,256]{1,0:T(1,128)S(1)}, f32[1,256,128]{2,1,0:T(8,128)S(1)})) conditional(s32[]{:T(128)} %convert_element_type.773, (f32[1,256]{1,0:T(1,128)S(1)}, f32[1,256]{1,0:T(1,128)S(1)}, f32[1,256,128]{2,1,0:T(8,128)S(1)}) %tuple.92, (s32[]{:T(128)}, s32[]{:T(128)}, bf16[16,512,1,128]{3,1,2,0:T(8,128)(2,1)}, ...), branch_computations={%region_2.2_spmd, %region_3.5_spmd} | conditional | flops 68487424 | bytes 2195534 | solution.py:197
  207.7 1.2 fusion.160
  210.3 1.3 dynamic_slice.93
  212.2 3.4 %conditional.3 = ((f32[1,256]{1,0:T(1,128)S(1)}, f32[1,256]{1,0:T(1,128)S(1)}, f32[1,256,128]{2,1,0:T(8,128)S(1)})) conditional(s32[]{:T(128)} %convert_element_type.773, (f32[1,256]{1,0:T(1,128)S(1)}, f32[1,256]{1,0:T(1,128)S(1)}, f32[1,256,128]{2,1,0:T(8,128)S(1)}) %tuple.92, (s32[]{:T(128)}, s32[]{:T(128)}, bf16[16,512,1,128]{3,1,2,0:T(8,128)(2,1)}, ...), branch_computations={%region_2.2_spmd, %region_3.5_spmd} | conditional | flops 68487424 | bytes 2195534 | solution.py:197
  215.7 1.3 dynamic_slice.93
  217.6 3.4 %conditional.3 = ((f32[1,256]{1,0:T(1,128)S(1)}, f32[1,256]{1,0:T(1,128)S(1)}, f32[1,256,128]{2,1,0:T(8,128)S(1)})) conditional(s32[]{:T(128)} %convert_element_type.773, (f32[1,256]{1,0:T(1,128)S(1)}, f32[1,256]{1,0:T(1,128)S(1)}, f32[1,256,128]{2,1,0:T(8,128)S(1)}) %tuple.92, (s32[]{:T(128)}, s32[]{:T(128)}, bf16[16,512,1,128]{3,1,2,0:T(8,128)(2,1)}, ...), branch_computations={%region_2.2_spmd, %region_3.5_spmd} | conditional | flops 68487424 | bytes 2195534 | solution.py:197
  221.0 1.3 dynamic_slice.93
  222.9 3.4 %conditional.3 = ((f32[1,256]{1,0:T(1,128)S(1)}, f32[1,256]{1,0:T(1,128)S(1)}, f32[1,256,128]{2,1,0:T(8,128)S(1)})) conditional(s32[]{:T(128)} %convert_element_type.773, (f32[1,256]{1,0:T(1,128)S(1)}, f32[1,256]{1,0:T(1,128)S(1)}, f32[1,256,128]{2,1,0:T(8,128)S(1)}) %tuple.92, (s32[]{:T(128)}, s32[]{:T(128)}, bf16[16,512,1,128]{3,1,2,0:T(8,128)(2,1)}, ...), branch_computations={%region_2.2_spmd, %region_3.5_spmd} | conditional | flops 68487424 | bytes 2195534 | solution.py:197
  226.3 1.3 dynamic_slice.93
  228.3 3.4 %conditional.3 = ((f32[1,256]{1,0:T(1,128)S(1)}, f32[1,256]{1,0:T(1,128)S(1)}, f32[1,256,128]{2,1,0:T(8,128)S(1)})) conditional(s32[]{:T(128)} %convert_element_type.773, (f32[1,256]{1,0:T(1,128)S(1)}, f32[1,256]{1,0:T(1,128)S(1)}, f32[1,256,128]{2,1,0:T(8,128)S(1)}) %tuple.92, (s32[]{:T(128)}, s32[]{:T(128)}, bf16[16,512,1,128]{3,1,2,0:T(8,128)(2,1)}, ...), branch_computations={%region_2.2_spmd, %region_3.5_spmd} | conditional | flops 68487424 | bytes 2195534 | solution.py:197
  229.0 1.2 fusion.160
  231.7 1.3 dynamic_slice.93
  234.4 2.2 fusion.50
  236.6 4.3 %all-to-all-start.1 = ((bf16[8,32,4096]{2,1,0:T(8,128)(2,1)}), bf16[8,32,4096]{2,1,0:T(8,128)(2,1)}, u32[]{:S(2)}, u32[]{:S(2)}) async-start(bf16[8,32,4096]{2,1,0:T(8,128)(2,1)} %bitcast.402), calls=%async_computation.1 | async-start | bytes 4194304 | tf_op jit(solution)/shard_map/all_to_all | solution.py:81
  241.6 26.6 %all-to-all-done.1 = bf16[8,32,4096]{2,1,0:T(8,128)(2,1)} async-done(((bf16[8,32,4096]{2,1,0:T(8,128)(2,1)}), bf16[8,32,4096]{2,1,0:T(8,128)(2,1)}, u32[]{:S(2)}, u32[]{:S(2)}) %all-to-all-start.1) | async-done | bytes 2097184 | tf_op jit(solution)/shard_map/all_to_all | solution.py:81
  268.2 2.7 reduce_sum.43
  (255 shorter events, 60.6 us)
Async XLA Ops:
  7.2 227.2 %copy-start = (bf16[256,4096]{1,0:T(8,128)(2,1)S(1)}, bf16[256,4096]{1,0:T(8,128)(2,1)}, u32[]{:S(2)}) copy-start(bf16[256,4096]{1,0:T(8,128)(2,1)} %param.35) | copy-start | bytes 6291460
  9.9 31.7 %all-to-all-start = ((bf16[8,256,512]{1,2,0:T(8,128)(2,1)}), bf16[8,256,512]{1,2,0:T(8,128)(2,1)}, u32[]{:S(2)}, u32[]{:S(2)}) async-start(bf16[8,256,512]{1,2,0:T(8,128)(2,1)} %broadcast_in_dim.45), calls=%async_computation | async-start | bytes 4194304 | tf_op jit(solution)/shard_map/all_to_all | solution.py:23
  14.3 29.5 %copy-start.9 = (f32[4096]{0:T(1024)S(1)}, f32[4096]{0:T(1024)}, u32[]{:S(2)}) copy-start(f32[4096]{0:T(1024)} %param.22) | copy-start | bytes 49156
  14.4 123.8 %all-gather.5.cloned.1.call-start = ((), (), s32[]{:S(2)}) async-start(), calls=%async_computation.2 | async-start | bytes 4325376 | tf_op jit(solution)/shard_map/all_gather | solution.py:42
  43.8 2.0 copy-start.14
  45.9 2.6 copy-start.1
  45.9 2.0 copy-start.15
  47.9 1.3 copy-start.4
  49.1 2.6 copy-start.2
  49.2 2.6 copy-start.5
  51.7 1.6 copy-start.13
  53.3 0.9 copy-start.8
  53.3 0.9 copy-start.10
  53.3 0.9 copy-start.12
  71.3 65.5 %copy-start.6 = (bf16[4096,128]{1,0:T(8,128)(2,1)S(1)}, bf16[4096,128]{1,0:T(8,128)(2,1)}, u32[]{:S(2)}) copy-start(bf16[4096,128]{1,0:T(8,128)(2,1)} %param.23) | copy-start | bytes 3145732
  72.1 64.7 %copy-start.3 = (bf16[256,4096]{0,1:T(8,128)(2,1)S(1)}, bf16[256,4096]{0,1:T(8,128)(2,1)}, u32[]{:S(2)}) copy-start(bf16[256,4096]{0,1:T(8,128)(2,1)} %copy-done.1) | copy-start | bytes 6291460
  151.5 82.1 %copy-start.7 = (bf16[128,4096]{1,0:T(8,128)(2,1)S(1)}, bf16[128,4096]{1,0:T(8,128)(2,1)}, u32[]{:S(2)}) copy-start(bf16[128,4096]{1,0:T(8,128)(2,1)} %param.34) | copy-start | bytes 3145732
  233.6 0.8 copy-start.11
  236.6 31.5 %all-to-all-start.1 = ((bf16[8,32,4096]{2,1,0:T(8,128)(2,1)}), bf16[8,32,4096]{2,1,0:T(8,128)(2,1)}, u32[]{:S(2)}, u32[]{:S(2)}) async-start(bf16[8,32,4096]{2,1,0:T(8,128)(2,1)} %bitcast.402), calls=%async_computation.1 | async-start | bytes 4194304 | tf_op jit(solution)/shard_map/all_to_all | solution.py:81
Sparse Core Ops, SparseCore 0:
  49.3 84.2 all-gather.4
where the time goes:
time: 282 us; the launch traced here: 278 us
  blocking collectives  62.8 us (22%)
  waiting for transfers between devices  52.5 us (19%)
  local copies, waits for them, and re-layouts  52.3 us (19%)
  matrix products  52.1 us (18%)
  other arithmetic  22.9 us (8%)
  between operations  14.4 us (5%)
  loops' own time  11.8 us (4%)
  starting transfers between devices  8.85 us (3%)
    all_gather x4, blocking collectives, carried_in(): lax.all_gather(part.astype(kind), axis)  62.8 us
    all_to_all x1, waiting for transfers between devices, summed_on_arrival(): lax.all_to_all(blocks, axis, split_axis=0, concat_axis=0, tiled=True)  26.6 us
    all_to_all x1, waiting for transfers between devices, from_everyone(): lax.all_to_all(jnp.broadcast_to(array[None], (size, *array.shape)), axis,...  25.9 us
    dynamic_slice x16, local copies, waits for them, and re-layouts, local(): lax.scan(inner, carry, (key_blocks, value_blocks, jnp.arange(span // sub,...  20.1 us
    dot_general x15, matrix products, work(): jnp.einsum('qhd,khd->hqk', queries, key_blk, preferred_element_type=jnp.f...  18.4 us
    dot_general x15, matrix products, work(): jnp.einsum('hqk,khd->hqd', weights.astype(jnp.bfloat16), value_blk, prefe...  18.2 us
    unnamed x35, local copies, waits for them, and re-layouts  11.8 us
    dynamic_slice x15, local copies, waits for them, and re-layouts, work(): k_cum = lax.dynamic_slice_in_dim(cum_gate, first, sub, 1)  11.4 us
  transfers between devices with their start and end apart: 3, of which 2 were waited for; matrix products, arithmetic and copies ran while one was open for 10% of the time, Pallas kernels for 0%

commit v1 on v0

v1 whole, which is shorter than its diff:
```python
import jax
import jax.numpy as jnp
from jax import lax
from jax.experimental import pallas as pl
from jax.experimental.pallas import tpu as pltpu
from jax.sharding import Mesh
from jax.sharding import PartitionSpec as P

MESH = pl.DeviceIdType.MESH
F32 = jnp.float32
BF16 = jnp.bfloat16

NZ, NX, NY, NC = 8, 4, 4, 2
TOK = 256
D = 4096
FEAT = 512
HEAD = 128
VAL = 256
EPS = 1e-06
TAU = 16.0
LOW = -3.0e38
KEY_SCALE = 128 ** (-0.5)

CHUNKS = 4
ROWS = TOK // CHUNKS
KV_CHUNKS = 4
KV_ROWS = TOK // KV_CHUNKS
COL_CHUNKS = 8
COLS = D // COL_CHUNKS
N_SEM = 160
N_LOC = 16


def nt(a, b):
    return lax.dot_general(a, b, (((1,), (1,)), ((), ())), preferred_element_type=F32)


def tn(a, b):
    return lax.dot_general(a, b, (((0,), (0,)), ((), ())), preferred_element_type=F32)


def mm(a, b):
    return jnp.dot(a, b, preferred_element_type=F32)


def iota(shape, dim):
    return lax.broadcasted_iota(jnp.int32, shape, dim)


def column_of(row):
    eye = iota((128, 128), 0) == iota((128, 128), 1)
    return jnp.sum(jnp.where(eye, row, 0.0), axis=1, keepdims=True)


def row_of(square):
    eye = iota((128, 128), 0) == iota((128, 128), 1)
    return jnp.sum(jnp.where(eye, square, 0.0), axis=0, keepdims=True)


def split3(value):
    high = value.astype(BF16)
    rest = value - high.astype(F32)
    mid = rest.astype(BF16)
    low = (rest - mid.astype(F32)).astype(BF16)
    return high, mid, low


def kernel(
    tokens,
    norm_gain,
    fox_query,
    fox_key,
    fox_value,
    cum_gate,
    lin_query,
    lin_key,
    lin_value,
    decay_down,
    decay_up,
    decay_bias,
    lin_gain,
    fox_out,
    lin_out,
    mixed,
    log_total,
    xg,
    w,
    wd,
    wo,
    acc,
    ssq,
    qs,
    kv,
    cq,
    top,
    oacc,
    ob,
    lb,
    op,
    lp,
    lcum,
    lout,
    qext,
    s1s,
    s1,
    s2,
    s3s,
    s3,
    heads,
    pb,
    pr,
    cb,
    raw,
    raws,
    fin,
    ss,
    rs,
    ls,
):
    z, x = lax.axis_index("z"), lax.axis_index("x")
    y, c = lax.axis_index("y"), lax.axis_index("c")
    other = 1 - c
    yp, ym, yo = lax.rem(y + 1, NY), lax.rem(y + 3, NY), lax.rem(y + 2, NY)
    zp, zm = lax.rem(z + 1, NZ), lax.rem(z + 7, NZ)
    sib = (z, x, y, other)
    up, down = (z, x, yp, c), (z, x, ym, c)
    z_up, z_down = (zp, x, y, c), (zm, x, y, c)

    sites = [0]
    pending = []

    def site():
        sites[0] += 1
        return sites[0] - 1

    def copy(src, dst, k, dev):
        return pltpu.make_async_remote_copy(
            src_ref=src,
            dst_ref=dst,
            send_sem=ss.at[k],
            recv_sem=rs.at[k],
            device_id=dev,
            device_id_type=MESH,
        )

    def send(src, dst, k, dev, when=None):
        if when is None:
            copy(src, dst, k, dev).start()
        else:
            pl.when(when)(lambda: copy(src, dst, k, dev).start())
        pending.append((src, dst, k, dev, when))

    def arrive(dst, k):
        copy(dst, dst, k, sib).wait_recv()

    own = y * 2 + c
    first = pltpu.make_async_copy(tokens, xg.at[own], ls.at[0])
    first.start()
    weights = []
    column = 0
    for n, ref in enumerate((fox_query, fox_key, fox_value, lin_query, lin_key, lin_value)):
        width = ref.shape[1]
        weights.append(pltpu.make_async_copy(ref, w.at[:, pl.ds(column, width)], ls.at[1 + n]))
        column += width
    weights.append(pltpu.make_async_copy(decay_down, wd, ls.at[7]))
    for item in weights:
        item.start()
    outs = [
        pltpu.make_async_copy(fox_out, wo.at[pl.ds(0, HEAD), :], ls.at[8]),
        pltpu.make_async_copy(lin_out, wo.at[pl.ds(HEAD, VAL), :], ls.at[9]),
    ]
    for item in outs:
        item.start()

    partners = [sib, up, down]
    partners += [(z, lax.rem(x + n, NX), y, c) for n in range(1, NX)]
    partners += [(lax.rem(z + n, NZ), x, y, c) for n in range(1, NZ)]
    barrier = pltpu.get_barrier_semaphore()
    for dev in partners:
        pl.semaphore_signal(barrier, inc=1, device_id=dev, device_id_type=MESH)
    pl.semaphore_wait(barrier, len(partners))

    first.wait()
    k_sib = site()
    k_up = [site() for _ in range(CHUNKS)]
    k_down = [site() for _ in range(CHUNKS)]
    k_far = [site() for _ in range(CHUNKS)]
    k_relay = [[site() for _ in range(CHUNKS)] for _ in range(3)]
    half = CHUNKS // 2

    def piece(block, n):
        return xg.at[block, pl.ds(n * ROWS, ROWS), :]

    def push(block, n, k, dev):
        send(piece(block, n), piece(block, n), k, dev)

    for n in range(CHUNKS):
        push(own, n, k_up[n], up)
        m = (n + half) % CHUNKS
        push(own, m, k_down[m], down)
    send(xg.at[own], xg.at[own], k_sib, sib)

    b_m, b_p, b_o = ym * 2 + c, yp * 2 + c, yo * 2 + c
    for item in weights:
        item.wait()
    w[:, pl.ds(896, 128)] = jnp.concatenate([wd[...], jnp.zeros((D, 112), BF16)], axis=1)
    acc[...] = jnp.zeros_like(acc)
    ssq[...] = jnp.zeros_like(ssq)

    def project(block):
        xb = xg[block].astype(F32)
        ssq[...] += jnp.sum(xb * xb, axis=1, keepdims=True)
        rows = pl.multiple_of(block * FEAT, FEAT)
        gain = norm_gain[:, pl.ds(rows, FEAT)]
        acc[...] += mm((xb * gain).astype(BF16), w[pl.ds(rows, FEAT), :])

    project(own)
    for n in range(half):
        m = n + half
        arrive(piece(b_m, n), k_up[n])
        push(b_m, n, k_far[n], up)
        push(b_m, n, k_relay[0][n], sib)
        arrive(piece(b_p, m), k_down[m])
        push(b_p, m, k_far[m], down)
        push(b_p, m, k_relay[1][m], sib)
    s_own, s_m, s_p, s_o = y * 2 + other, ym * 2 + other, yp * 2 + other, yo * 2 + other
    arrive(xg.at[s_own], k_sib)
    project(s_own)
    for n in range(half):
        m = n + half
        arrive(piece(b_m, m), k_up[m])
        push(b_m, m, k_relay[0][m], sib)
        arrive(piece(b_p, n), k_down[n])
        push(b_p, n, k_relay[1][n], sib)
    lax.fori_loop(0, 2, lambda i, _: project(jnp.where(i == 0, b_m, b_p)), None)
    for n in range(half):
        m = n + half
        arrive(piece(b_o, n), k_far[n])
        push(b_o, n, k_relay[2][n], sib)
        arrive(piece(b_o, m), k_far[m])
        push(b_o, m, k_relay[2][m], sib)
    for n in range(CHUNKS):
        arrive(piece(s_m, n), k_relay[0][n])
        arrive(piece(s_p, n), k_relay[1][n])

    def late(i, _):
        project(jnp.where(i == 0, s_m, jnp.where(i == 1, s_p, b_o)))

    lax.fori_loop(0, 3, late, None)
    for n in range(CHUNKS):
        arrive(piece(s_o, n), k_relay[2][n])
    project(s_o)

    norm = lax.rsqrt(ssq[:, 0:1] * (1.0 / D) + EPS)

    def result(start, width):
        return acc[:, pl.ds(start, width)] * norm

    qs[x] = (result(0, 128) * HEAD ** (-0.5)).astype(BF16)
    kv[z] = result(128, 256).astype(BF16)

    kv_half = KV_CHUNKS // 2

    def reach(n):
        return (4, 3) if n < kv_half else (3, 4)

    k_kv = {}
    for step in range(1, 5):
        for n in range(KV_CHUNKS):
            for way in (0, 1):
                if step <= reach(n)[way]:
                    k_kv[step, n, way] = site()

    def origin(step, way):
        return lax.rem(z + (NZ - step if way == 0 else step), NZ)

    def kv_piece(block, n):
        return kv.at[block, pl.ds(n * KV_ROWS, KV_ROWS), :]

    def kv_send(step, n, way):
        if (step, n, way) in k_kv:
            part = kv_piece(origin(step - 1, way), n)
            send(part, part, k_kv[step, n, way], z_down if way else z_up)

    def ring(step):
        for m in range(kv_half):
            for n, way in ((m, 0), (m + kv_half, 1)):
                arrive(kv_piece(origin(step, way), n), k_kv[step, n, way])
                kv_send(step + 1, n, way)
        for m in range(kv_half):
            for n, way in ((m + kv_half, 0), (m, 1)):
                if (step, n, way) in k_kv:
                    arrive(kv_piece(origin(step, way), n), k_kv[step, n, way])
                    kv_send(step + 1, n, way)

    for m in range(kv_half):
        kv_send(1, m, 0)
        kv_send(1, m + kv_half, 1)
    for m in range(kv_half):
        kv_send(1, m + kv_half, 0)
        kv_send(1, m, 1)

    def x_at(n):
        return lax.rem(x + n, NX)

    k_q = [site() for _ in range(NX)]
    for n in range(1, NX):
        send(qs.at[x], qs.at[x], k_q[n], (z, x_at(n), y, c))

    lk = result(512, 128).astype(BF16).astype(F32)
    lv = result(640, 256).astype(BF16)
    low = result(896, 128).astype(BF16)
    up_weight = jnp.concatenate([decay_up[...], jnp.zeros((112, 128), BF16)], axis=0)
    pre = mm(low, up_weight) + decay_bias[...]
    decay = (jnp.minimum(pre, 0.0) - jnp.log1p(jnp.exp(-jnp.abs(pre)))) * (1.0 / TAU)
    lower = (iota((TOK, TOK), 0) >= iota((TOK, TOK), 1)).astype(BF16)
    sums = mm(lower, jnp.concatenate(split3(decay), axis=1))
    cum = sums[:, 0:128] + sums[:, 128:256] + sums[:, 256:384]
    lcum[...] = cum
    last = cum[TOK - 1 : TOK, :]
    state = tn(lv, (lk * jnp.exp(last - cum)).astype(BF16))
    quarter = VAL // NX
    row16 = iota((16, 128), 0)

    def pack(ref, values, total):
        ref[pl.ds(0, quarter), :] = values.astype(BF16)
        parts = split3(total)
        tail = jnp.zeros((16, 128), F32)
        for n in range(3):
            tail = jnp.where(row16 == n, parts[n].astype(F32), tail)
        ref[pl.ds(quarter, 16), :] = tail.astype(BF16)

    def unpack(ref):
        values = ref[pl.ds(0, quarter), :].astype(F32)
        tail = ref[pl.ds(quarter, 16), :].astype(F32)
        total = tail[0:1, :] + tail[1:2, :] + tail[2:3, :]
        return values, total

    for n in range(NX):
        pack(s1s.at[n], state[n * quarter : (n + 1) * quarter, :], last)
    k_s1 = [site() for _ in range(NX)]
    for n in range(1, NX):
        send(s1s.at[x_at(n)], s1.at[x], k_s1[n], (z, x_at(n), y, c))

    ring(1)

    lq = result(384, 128).astype(BF16).astype(F32) * KEY_SCALE
    qext[...] = (lq * jnp.exp(cum)).astype(BF16)
    rows_i, cols_j = iota((TOK, TOK), 0), iota((TOK, TOK), 1)
    row_id = iota((TOK, HEAD), 0)
    grouped = (TOK // 8, 8, HEAD)
    q8, k8, c8 = lq.reshape(grouped), lk.reshape(grouped), cum.reshape(grouped)
    place = iota(grouped, 1)
    total = jnp.zeros((TOK, TOK), F32)
    for back in range(8):
        if back:
            gap = jnp.where(place >= back, c8 - pltpu.roll(c8, back, 1), -jnp.inf)
            product = q8 * pltpu.roll(k8, back, 1) * jnp.exp(gap)
        else:
            product = q8 * k8
        one = jnp.sum(product.reshape(TOK, HEAD), axis=1, keepdims=True)
        total = jnp.where(rows_i - cols_j == back, one, total)
    span = 8
    while span < TOK:
        pairs = (TOK // (2 * span), 2 * span, HEAD)
        edge = jnp.broadcast_to(cum.reshape(pairs)[:, span - 1 : span, :], pairs).reshape(TOK, HEAD)
        right = (row_id // span) % 2 == 1
        fall = jnp.exp(-jnp.abs(cum - edge))
        q_part = jnp.where(right, lq * fall, 0.0).astype(BF16)
        k_part = jnp.where(right, 0.0, lk * fall).astype(BF16)
        same = rows_i // (2 * span) == cols_j // (2 * span)
        total = total + jnp.where(same, nt(q_part, k_part), 0.0)
        span *= 2
    lout[...] = mm(total.astype(BF16), lv)

    for n in range(1, NX):
        arrive(qs.at[x_at(NX - n)], k_q[n])
    for j in range(NX):
        for n in range(2):
            start = pl.multiple_of((z * NX + j) * TOK + n * 128, 128)
            column_gate = column_of(cum_gate[:, pl.ds(start, 128)])
            cq[j, pl.ds(n * 128, 128), :] = jnp.broadcast_to(column_gate, (128, 128))

    def logits(j, block):
        start = pl.multiple_of((block * NX + x) * TOK, TOK)
        gate = cum_gate[:, pl.ds(start, TOK)]
        return nt(qs[j], kv[block, :, pl.ds(0, HEAD)]) + (cq[j][:, 0:1] - gate)

    def values(block):
        return jnp.concatenate(
            [kv[block, :, pl.ds(HEAD, HEAD)], jnp.ones((TOK, HEAD), BF16)], axis=1
        )

    def diagonal(j, _):
        seen = iota((TOK, TOK), 1) + x * TOK <= iota((TOK, TOK), 0) + j * TOK
        logit = jnp.where(seen, logits(j, z), LOW)
        peak = jnp.max(logit, axis=1, keepdims=True)
        top[j] = jnp.broadcast_to(peak, (TOK, HEAD))
        oacc[j] = mm(jnp.exp(logit - peak).astype(BF16), values(z))

    lax.fori_loop(0, NX, diagonal, None)

    def attend(block):
        def one(j, _):
            logit = logits(j, block)
            old = top[j][:, 0:1]
            peak = jnp.maximum(old, jnp.max(logit, axis=1, keepdims=True))
            top[j] = jnp.broadcast_to(peak, (TOK, HEAD))
            weight = jnp.exp(logit - peak).astype(BF16)
            oacc[j] = oacc[j] * jnp.exp(old - peak) + mm(weight, values(block))

        pl.when(block < z)(lambda: lax.fori_loop(0, NX, one, None))

    def attend_both(step):
        def one(way, _):
            attend(lax.rem(z + jnp.where(way == 0, NZ - step, step), NZ))

        lax.fori_loop(0, 2, one, None)

    ring(2)
    attend_both(1)

    for n in range(1, NX):
        arrive(s1.at[x_at(NX - n)], k_s1[n])
    s1[x] = s1s[x]
    row_state, row_total = jnp.zeros((quarter, 128), F32), jnp.zeros((1, 128), F32)
    for n in range(NX):
        values_n, total_n = unpack(s1.at[n])
        row_state = jnp.exp(total_n) * row_state + values_n
        row_total = row_total + total_n
    pack(s2.at[z], row_state, row_total)
    k_s2 = [site() for _ in range(NZ)]
    for n in range(1, NZ):
        send(s2.at[z], s2.at[z], k_s2[n], (lax.rem(z + n, NZ), x, y, c), when=z + n < NZ)

    ring(3)
    attend_both(2)

    for n in range(1, NZ):
        before = lax.rem(z + NZ - n, NZ)
        pl.when(z >= n)(lambda before=before, n=n: arrive(s2.at[before], k_s2[n]))

    def earlier(n, state):
        values_n, total_n = unpack(s2.at[n])
        return jnp.exp(total_n) * state + values_n

    state = lax.fori_loop(0, z, earlier, jnp.zeros((quarter, 128), F32))
    for n in range(NX):
        s3s[n] = state.astype(BF16)
        values_n, total_n = unpack(s1.at[n])
        state = jnp.exp(total_n) * state + values_n
    k_s3 = [site() for _ in range(NX)]
    for n in range(1, NX):
        send(s3s.at[x_at(n)], s3.at[x], k_s3[n], (z, x_at(n), y, c))

    ring(4)
    attend_both(3)
    attend(lax.rem(z + 4, NZ))

    def close(j, _):
        mass = oacc[j][:, HEAD:]
        op[j] = (oacc[j][:, 0:HEAD] / mass).astype(BF16)
        height = top[j] + jnp.log(mass)
        first_row, second_row = row_of(height[0:128]), row_of(height[128:256])
        row8 = iota((8, 128), 0)
        lp[j] = jnp.where(row8 == 0, first_row, jnp.where(row8 == 1, second_row, 0.0))

    lax.fori_loop(0, NX, close, None)
    k_o = [site() for _ in range(NX)]
    k_l = [site() for _ in range(NX)]
    for n in range(1, NX):
        dev = (z, x_at(n), y, c)
        send(op.at[x_at(n)], ob.at[x], k_o[n], dev)
        send(lp.at[x_at(n)], lb.at[x], k_l[n], dev)

    for n in range(1, NX):
        arrive(s3.at[x_at(NX - n)], k_s3[n])
    s3[x] = s3s[x]
    whole = jnp.concatenate([s3[n] for n in range(NX)], axis=0)
    lin_raw = lout[...] + nt(qext[...], whole)
    mean = jnp.mean(lin_raw * lin_raw, axis=1, keepdims=True)
    heads[:, pl.ds(HEAD, VAL)] = (lin_raw * lax.rsqrt(mean + EPS) * lin_gain[...]).astype(BF16)

    for n in range(1, NX):
        arrive(ob.at[x_at(NX - n)], k_o[n])
        arrive(lb.at[x_at(NX - n)], k_l[n])
    ob[x] = op[x]
    lb[x] = lp[x]
    heights = [lb[n] for n in range(NX)]
    peak = jnp.maximum(jnp.maximum(heights[0], heights[1]), jnp.maximum(heights[2], heights[3]))
    shares = [jnp.exp(h - peak) for h in heights]
    mass = shares[0] + shares[1] + shares[2] + shares[3]
    summit = peak + jnp.log(mass)
    for n in range(2):
        rows = pl.ds(n * 128, 128)
        log_total[:, rows] = summit[n : n + 1, :]
        mix = jnp.zeros((128, HEAD), F32)
        for m in range(NX):
            share = column_of((shares[m] / mass)[n : n + 1, :])
            mix = mix + share * ob[m, rows, :].astype(F32)
        heads[rows, pl.ds(0, HEAD)] = mix.astype(BF16)

    for item in outs:
        item.wait()
    k_pair = [site() for _ in range(COL_CHUNKS)]
    k_raw = [site() for _ in range(COL_CHUNKS)]
    k_fin = [[site() for _ in range(2)] for _ in range(COL_CHUNKS)]
    col_half = COL_CHUNKS // 2
    order = [n + half_n for n in range(col_half) for half_n in (0, col_half)]

    def produce(n):
        part = mm(heads[...], wo[:, pl.ds(n * COLS, COLS)]).astype(BF16)
        part = part.reshape(NY, NC, 32, COLS)
        for m in range(NC):
            pb[n, m] = part[:, m]
        send(pb.at[n, other], pr.at[n], k_pair[n], sib)

    def spread(n):
        arrive(pr.at[n], k_pair[n])
        cb[n] = (pb[n, c].astype(F32) + pr[n].astype(F32)).astype(BF16)
        near, far = (down, up) if n < col_half else (up, down)
        y_near = ym if n < col_half else yp
        send(cb.at[n, yo], raw.at[n], k_raw[n], far)
        send(cb.at[n, y_near], fin.at[n, 1], k_fin[n][1], near)

    def relay(n):
        arrive(raw.at[n], k_raw[n])
        far, y_far = (up, yp) if n < col_half else (down, ym)
        raws[n] = (cb[n, y_far].astype(F32) + raw[n].astype(F32)).astype(BF16)
        send(raws.at[n], fin.at[n, 0], k_fin[n][0], far)

    def finish(n):
        for m in range(2):
            arrive(fin.at[n, m], k_fin[n][m])
        done = cb[n, y].astype(F32) + fin[n, 0].astype(F32) + fin[n, 1].astype(F32)
        mixed[:, pl.ds(n * COLS, COLS)] = done.astype(BF16)

    for i in range(COL_CHUNKS + 1):
        if i < COL_CHUNKS:
            produce(order[i])
        if i:
            spread(order[i - 1])
    for n in order:
        relay(n)
    for n in order:
        finish(n)

    for src, dst, k, dev, when in pending:
        if when is None:
            copy(src, dst, k, dev).wait_send()
        else:
            pl.when(when)(lambda a=(src, dst, k, dev): copy(*a).wait_send())


def vmem(shape, dtype):
    return pltpu.VMEM(shape, dtype)


SCRATCH = [
    vmem((NY * NC, TOK, FEAT), BF16),
    vmem((D, 1024), BF16),
    vmem((D, 16), BF16),
    vmem((HEAD + VAL, D), BF16),
    vmem((TOK, 1024), F32),
    vmem((TOK, 128), F32),
    vmem((NX, TOK, HEAD), BF16),
    vmem((NZ, TOK, 2 * HEAD), BF16),
    vmem((NX, TOK, 128), F32),
    vmem((NX, TOK, 128), F32),
    vmem((NX, TOK, 2 * HEAD), F32),
    vmem((NX, TOK, HEAD), BF16),
    vmem((NX, 8, 128), F32),
    vmem((NX, TOK, HEAD), BF16),
    vmem((NX, 8, 128), F32),
    vmem((TOK, 128), F32),
    vmem((TOK, VAL), F32),
    vmem((TOK, 128), BF16),
    vmem((NX, VAL // NX + 16, 128), BF16),
    vmem((NX, VAL // NX + 16, 128), BF16),
    vmem((NZ, VAL // NX + 16, 128), BF16),
    vmem((NX, VAL // NX, 128), BF16),
    vmem((NX, VAL // NX, 128), BF16),
    vmem((TOK, HEAD + VAL), BF16),
    vmem((COL_CHUNKS, NC, NY, 32, COLS), BF16),
    vmem((COL_CHUNKS, NY, 32, COLS), BF16),
    vmem((COL_CHUNKS, NY, 32, COLS), BF16),
    vmem((COL_CHUNKS, 32, COLS), BF16),
    vmem((COL_CHUNKS, 32, COLS), BF16),
    vmem((COL_CHUNKS, 2, 32, COLS), BF16),
    pltpu.SemaphoreType.DMA((N_SEM,)),
    pltpu.SemaphoreType.DMA((N_SEM,)),
    pltpu.SemaphoreType.DMA((N_LOC,)),
]


def local(
    tokens,
    norm_gain,
    fox_query,
    fox_key,
    fox_value,
    cum_gate,
    lin_query,
    lin_key,
    lin_value,
    decay_down,
    decay_up,
    decay_bias,
    lin_gain,
    fox_out,
    lin_out,
):
    here = pl.BlockSpec(memory_space=pltpu.VMEM)
    far = pl.BlockSpec(memory_space=pl.ANY)
    specs = [far, here, far, far, far, here, far, far, far, far, here, here, here, far, far]
    return pl.pallas_call(
        kernel,
        name="layer",
        out_shape=(
            jax.ShapeDtypeStruct((32, D), BF16),
            jax.ShapeDtypeStruct((1, TOK), F32),
        ),
        in_specs=specs,
        out_specs=(here, here),
        scratch_shapes=SCRATCH,
        compiler_params=pltpu.CompilerParams(
            collective_id=0, has_side_effects=True, vmem_limit_bytes=60 * 1024 * 1024
        ),
    )(
        tokens,
        norm_gain.reshape(1, D),
        fox_query,
        fox_key,
        fox_value,
        cum_gate,
        lin_query,
        lin_key,
        lin_value,
        decay_down,
        decay_up,
        decay_bias.reshape(1, HEAD),
        lin_gain.reshape(1, VAL),
        fox_out,
        lin_out,
    )


def solution(mesh):
    torus = Mesh(mesh.devices.reshape(NZ, NX, NY, NC), ("z", "x", "y", "c"))
    sp, tp, sp_tp = ("z", "x"), ("y", "c"), ("z", "x", "y", "c")
    in_specs = (
        P(sp, tp),
        P(),
        P(None, tp),
        P(None, tp),
        P(None, tp),
        P(tp, None),
        P(None, tp),
        P(None, tp),
        P(None, tp),
        P(),
        P(None, tp),
        P(tp),
        P(),
        P(tp, None),
        P(tp, None),
    )
    out_specs = (P(sp_tp, None), P(tp, sp))
    return jax.shard_map(local, mesh=torus, in_specs=in_specs, out_specs=out_specs, check_vma=False)
```

time: 282 us -> 74.5 us (0.26); the launches traced: 278 us -> 74.3 us
  Pallas kernels: 0 us -> 68.6 us
  blocking collectives: 62.8 us -> 0 us
  waiting for transfers between devices: 52.5 us -> 0 us
  matrix products: 52.1 us -> 0 us
  local copies, waits for them, and re-layouts: 52.3 us -> 5.1 us
  other arithmetic: 22.9 us -> 0 us
  between operations: 14.4 us -> 0.64 us
  loops' own time: 11.8 us -> 0 us
  starting transfers between devices: 8.85 us -> 0 us
    pallas_call x0 -> x1, Pallas kernels: none -> 68.6 us  [local(): pl.pallas_call(kernel, name='layer', out_shape=(jax.ShapeDtypeStruct((32,...]
    all_gather x4 -> x0, blocking collectives: 62.8 us -> none  [carried_in(): lax.all_gather(part.astype(kind), axis)]
    all_to_all x2 -> x0, waiting for transfers between devices: 52.5 us -> none  [the longest x1 26.6 us: summed_on_arrival(): lax.all_to_all(blocks, axis, split_axis=0, concat_axis=0, tiled=True)]
    dot_general x52 -> x0, matrix products: 52.1 us -> none  [the longest x15 18.4 us: work(): jnp.einsum('qhd,khd->hqk', queries, key_blk, preferred_element_type=jnp.f...]
    dynamic_slice x32 -> x0, local copies, waits for them, and re-layouts: 32.8 us -> none  [the longest x16 20.1 us: local(): lax.scan(inner, carry, (key_blocks, value_blocks, jnp.arange(span // sub,...]
    another operation x18 -> x0, loops' own time: 11.8 us -> none  [the longest x1 10.8 us: local(): lax.scan(inner, carry, (key_blocks, value_blocks, jnp.arange(span // sub,...]
    all_to_all x2 -> x0, starting transfers between devices: 8.81 us -> none  [the longest x1 4.47 us: from_everyone(): lax.all_to_all(jnp.broadcast_to(array[None], (size, *array.shape)), axis,...]
    dot_general x4 -> x0, other arithmetic: 6.84 us -> none  [block_step(): scores = jnp.einsum('id,jd,ijd->ij', q_b, k_b, decay)]
  transfers between devices with their start and end apart: 3 -> 0, of which waited for: 2 -> 0; matrix products, arithmetic and copies ran while one was open for 10% -> 0% of each run, Pallas kernels for 0% -> 0%
where the time goes in v1:
time: 74.5 us; the launch traced here: 74.3 us
  Pallas kernels  68.6 us (92%)
  local copies, waits for them, and re-layouts  5.1 us (7%)
    pallas_call x1, Pallas kernels, local(): pl.pallas_call(kernel, name='layer', out_shape=(jax.ShapeDtypeStruct((32,...  68.6 us
    unnamed x3, local copies, waits for them, and re-layouts  5.1 us

profile of v1, /device:TPU:224, one launch (start us, length us, event | category | flops | bytes accessed | tf_op | source)
XLA Modules:
  0.0 74.3 jit_solution(9601315317894266571)
XLA Ops:
  0.6 2.2 %copy.17.decay_down = bf16[4096,16]{1,0:T(8,128)(2,1)} copy(bf16[4096,16]{0,1:T(8,128)(2,1)} %param.24) | data formatting | bytes 262144 | tf_op args[9]
  2.9 68.6 %layer.1 = (bf16[32,4096]{1,0:T(8,128)(2,1)}, f32[1,256]{1,0:T(1,128)}) custom-call(bf16[256,512]{1,0:T(8,128)(2,1)} %tokens.1, f32[1,4096]{1,0:T(1,128)} %bitcast.3, bf16[4096,128]{1,0:T(8,128)(2,1)} %fox_query.1, bf16[4096,128]{1,0:T(8,128)(2,1)} %fox_key.1, bf16[4096,128]{1,0:T(8,128)(2,1)} %fox_value.1, f32[1,8192]{1,0:T(1,128)} %cum_gate.1, ...), custom_call_target="tpu_custom_call" | custom-call | tf_op jit(solution)/shard_map/layer/pallas_call | solution.py:616
  71.5 1.7 %copy.20 = bf16[32,4096]{1,0:T(8,128)(2,1)} copy(bf16[32,4096]{1,0:T(8,128)(2,1)} %get-tuple-element.4) | data formatting | bytes 524288
  73.1 1.2 %copy.21 = f32[1,256]{1,0:T(1,128)} copy(f32[1,256]{1,0:T(1,128)} %get-tuple-element.5) | data formatting | bytes 2048

commit v2 on v1

--- a/solution.py
+++ b/solution.py
@@ -67,21 +67,22 @@
 
 def kernel(
     tokens,
-    norm_gain,
+    norm_gain_far,
     fox_query,
     fox_key,
     fox_value,
-    cum_gate,
+    cum_gate_far,
     lin_query,
     lin_key,
     lin_value,
     decay_down,
-    decay_up,
-    decay_bias,
-    lin_gain,
+    decay_up_far,
+    decay_bias_far,
+    lin_gain_far,
     fox_out,
     lin_out,
-    mixed,
+    own_part,
+    fin,
     log_total,
     xg,
     w,
@@ -98,6 +99,7 @@
     lb,
     op,
     lp,
+    share,
     lcum,
     lout,
     qext,
@@ -112,7 +114,11 @@
     cb,
     raw,
     raws,
-    fin,
+    norm_gain,
+    cum_gate,
+    decay_up,
+    decay_bias,
+    lin_gain,
     ss,
     rs,
     ls,
@@ -163,6 +169,14 @@
         weights.append(pltpu.make_async_copy(ref, w.at[:, pl.ds(column, width)], ls.at[1 + n]))
         column += width
     weights.append(pltpu.make_async_copy(decay_down, wd, ls.at[7]))
+    smalls = [
+        pltpu.make_async_copy(norm_gain_far, norm_gain, ls.at[10]),
+        pltpu.make_async_copy(cum_gate_far, cum_gate, ls.at[11]),
+        pltpu.make_async_copy(decay_up_far, decay_up, ls.at[12]),
+        pltpu.make_async_copy(decay_bias_far, decay_bias, ls.at[13]),
+        pltpu.make_async_copy(lin_gain_far, lin_gain, ls.at[14]),
+    ]
+    weights = smalls + weights
     for item in weights:
         item.start()
     outs = [
@@ -174,7 +188,8 @@
 
     partners = [sib, up, down]
     partners += [(z, lax.rem(x + n, NX), y, c) for n in range(1, NX)]
-    partners += [(lax.rem(z + n, NZ), x, y, c) for n in range(1, NZ)]
+    z_four = (lax.rem(z + 4, NZ), x, y, c)
+    partners += [z_up, z_down, z_four]
     barrier = pltpu.get_barrier_semaphore()
     for dev in partners:
         pl.semaphore_signal(barrier, inc=1, device_id=dev, device_id_type=MESH)
@@ -203,7 +218,13 @@
     b_m, b_p, b_o = ym * 2 + c, yp * 2 + c, yo * 2 + c
     for item in weights:
         item.wait()
-    w[:, pl.ds(896, 128)] = jnp.concatenate([wd[...], jnp.zeros((D, 112), BF16)], axis=1)
+
+    def widen(i, _):
+        rows = pl.ds(pl.multiple_of(i * FEAT, FEAT), FEAT)
+        part = jnp.concatenate([wd[:, rows].astype(F32), jnp.zeros((112, FEAT), F32)], axis=0)
+        w[rows, pl.ds(896, 128)] = part.T.astype(BF16)
+
+    lax.fori_loop(0, NY * NC, widen, None)
     acc[...] = jnp.zeros_like(acc)
     ssq[...] = jnp.zeros_like(ssq)
 
@@ -232,21 +253,20 @@
         push(b_m, m, k_relay[0][m], sib)
         arrive(piece(b_p, n), k_down[n])
         push(b_p, n, k_relay[1][n], sib)
-    lax.fori_loop(0, 2, lambda i, _: project(jnp.where(i == 0, b_m, b_p)), None)
+    project(b_m)
+    project(b_p)
+    late_blocks = (s_m, s_p)
     for n in range(half):
         m = n + half
         arrive(piece(b_o, n), k_far[n])
         push(b_o, n, k_relay[2][n], sib)
         arrive(piece(b_o, m), k_far[m])
         push(b_o, m, k_relay[2][m], sib)
-    for n in range(CHUNKS):
-        arrive(piece(s_m, n), k_relay[0][n])
-        arrive(piece(s_p, n), k_relay[1][n])
-
-    def late(i, _):
-        project(jnp.where(i == 0, s_m, jnp.where(i == 1, s_p, b_o)))
-
-    lax.fori_loop(0, 3, late, None)
+        if n < 2:
+            for r in range(CHUNKS):
+                arrive(piece(late_blocks[n], r), k_relay[n][r])
+            project(late_blocks[n])
+    project(b_o)
     for n in range(CHUNKS):
         arrive(piece(s_o, n), k_relay[2][n])
     project(s_o)
@@ -277,21 +297,30 @@
     def kv_piece(block, n):
         return kv.at[block, pl.ds(n * KV_ROWS, KV_ROWS), :]
 
+    def wanted(step, n, way, receiver):
+        if way == 0:
+            return receiver >= step
+        far = receiver + step
+        return jnp.logical_or(far >= NZ, far + 1 <= reach(n)[1])
+
     def kv_send(step, n, way):
         if (step, n, way) in k_kv:
             part = kv_piece(origin(step - 1, way), n)
-            send(part, part, k_kv[step, n, way], z_down if way else z_up)
-
-    def ring(step):
-        for m in range(kv_half):
-            for n, way in ((m, 0), (m + kv_half, 1)):
-                arrive(kv_piece(origin(step, way), n), k_kv[step, n, way])
-                kv_send(step + 1, n, way)
-        for m in range(kv_half):
-            for n, way in ((m + kv_half, 0), (m, 1)):
-                if (step, n, way) in k_kv:
-                    arrive(kv_piece(origin(step, way), n), k_kv[step, n, way])
-                    kv_send(step + 1, n, way)
+            dev, receiver = (z_down, zm) if way else (z_up, zp)
+            send(part, part, k_kv[step, n, way], dev, wanted(step, n, way, receiver))
+
+    def kv_step(step, n, way):
+        if (step, n, way) in k_kv:
+            part = kv_piece(origin(step, way), n)
+            k = k_kv[step, n, way]
+            pl.when(wanted(step, n, way, z))(lambda: arrive(part, k))
+            kv_send(step + 1, n, way)
+
+    def slot(step, number):
+        m = number % kv_half
+        pairs = ((m, 0), (m + kv_half, 1)) if number < kv_half else ((m + kv_half, 0), (m, 1))
+        for n, way in pairs:
+            kv_step(step, n, way)
 
     for m in range(kv_half):
         kv_send(1, m, 0)
@@ -302,10 +331,6 @@
 
     def x_at(n):
         return lax.rem(x + n, NX)
-
-    k_q = [site() for _ in range(NX)]
-    for n in range(1, NX):
-        send(qs.at[x], qs.at[x], k_q[n], (z, x_at(n), y, c))
 
     lk = result(512, 128).astype(BF16).astype(F32)
     lv = result(640, 256).astype(BF16)
@@ -342,7 +367,9 @@
     for n in range(1, NX):
         send(s1s.at[x_at(n)], s1.at[x], k_s1[n], (z, x_at(n), y, c))
 
-    ring(1)
+    k_q = [site() for _ in range(NX)]
+    for n in range(1, NX):
+        send(qs.at[x], qs.at[x], k_q[n], (z, x_at(n), y, c))
 
     lq = result(384, 128).astype(BF16).astype(F32) * KEY_SCALE
     qext[...] = (lq * jnp.exp(cum)).astype(BF16)
@@ -373,8 +400,6 @@
         span *= 2
     lout[...] = mm(total.astype(BF16), lv)
 
-    for n in range(1, NX):
-        arrive(qs.at[x_at(NX - n)], k_q[n])
     for j in range(NX):
         for n in range(2):
             start = pl.multiple_of((z * NX + j) * TOK + n * 128, 128)
@@ -384,41 +409,45 @@
     def logits(j, block):
         start = pl.multiple_of((block * NX + x) * TOK, TOK)
         gate = cum_gate[:, pl.ds(start, TOK)]
-        return nt(qs[j], kv[block, :, pl.ds(0, HEAD)]) + (cq[j][:, 0:1] - gate)
+        own_gate = cq[j]
+        own_gate = jnp.concatenate([own_gate, own_gate], axis=1)
+        return nt(qs[j], kv[block, :, pl.ds(0, HEAD)]) + (own_gate - gate)
 
     def values(block):
         return jnp.concatenate(
             [kv[block, :, pl.ds(HEAD, HEAD)], jnp.ones((TOK, HEAD), BF16)], axis=1
         )
 
-    def diagonal(j, _):
-        seen = iota((TOK, TOK), 1) + x * TOK <= iota((TOK, TOK), 0) + j * TOK
-        logit = jnp.where(seen, logits(j, z), LOW)
-        peak = jnp.max(logit, axis=1, keepdims=True)
-        top[j] = jnp.broadcast_to(peak, (TOK, HEAD))
-        oacc[j] = mm(jnp.exp(logit - peak).astype(BF16), values(z))
-
-    lax.fori_loop(0, NX, diagonal, None)
-
-    def attend(block):
-        def one(j, _):
+    def diagonal(some):
+        mine = values(z)
+        for j in some:
+            seen = iota((TOK, TOK), 1) + x * TOK <= iota((TOK, TOK), 0) + j * TOK
+            logit = jnp.where(seen, logits(j, z), LOW)
+            peak = jnp.max(logit, axis=1, keepdims=True)
+            top[j] = jnp.broadcast_to(peak, (TOK, HEAD))
+            oacc[j] = mm(jnp.exp(logit - peak).astype(BF16), mine)
+
+    def update(block, some):
+        theirs = values(block)
+        for j in some:
             logit = logits(j, block)
-            old = top[j][:, 0:1]
+            old = top[j]
             peak = jnp.maximum(old, jnp.max(logit, axis=1, keepdims=True))
-            top[j] = jnp.broadcast_to(peak, (TOK, HEAD))
-            weight = jnp.exp(logit - peak).astype(BF16)
-            oacc[j] = oacc[j] * jnp.exp(old - peak) + mm(weight, values(block))
-
-        pl.when(block < z)(lambda: lax.fori_loop(0, NX, one, None))
-
-    def attend_both(step):
-        def one(way, _):
-            attend(lax.rem(z + jnp.where(way == 0, NZ - step, step), NZ))
-
-        lax.fori_loop(0, 2, one, None)
-
-    ring(2)
-    attend_both(1)
+            top[j] = peak
+            wide = jnp.concatenate([peak, peak], axis=1)
+            weight = jnp.exp(logit - wide).astype(BF16)
+            fade = jnp.exp(old - peak)
+            fade = jnp.concatenate([fade, fade], axis=1)
+            oacc[j] = oacc[j] * fade + mm(weight, theirs)
+
+    def attend(step, way):
+        block = origin(step, way)
+        pl.when(block < z)(lambda: update(block, range(NX)))
+
+    slot(1, 0)
+    slot(1, 1)
+    slot(1, 2)
+    slot(1, 3)
 
     for n in range(1, NX):
         arrive(s1.at[x_at(NX - n)], k_s1[n])
@@ -429,16 +458,69 @@
         row_state = jnp.exp(total_n) * row_state + values_n
         row_total = row_total + total_n
     pack(s2.at[z], row_state, row_total)
-    k_s2 = [site() for _ in range(NZ)]
-    for n in range(1, NZ):
-        send(s2.at[z], s2.at[z], k_s2[n], (lax.rem(z + n, NZ), x, y, c), when=z + n < NZ)
-
-    ring(3)
-    attend_both(2)
-
-    for n in range(1, NZ):
-        before = lax.rem(z + NZ - n, NZ)
-        pl.when(z >= n)(lambda before=before, n=n: arrive(s2.at[before], k_s2[n]))
+    k_s2 = {(step, way): site() for step in range(1, 4) for way in (0, 1)}
+    k_far_state = site()
+
+    def state_send(step, way):
+        if (step, way) in k_s2:
+            dev, receiver = (z_down, zm) if way else (z_up, zp)
+            part = s2.at[origin(step - 1, way)]
+            send(part, part, k_s2[step, way], dev, wanted(step, 0, way, receiver))
+
+    def state_step(step):
+        for way in (0, 1):
+            if (step, way) in k_s2:
+                part, k = s2.at[origin(step, way)], k_s2[step, way]
+                pl.when(wanted(step, 0, way, z))(lambda part=part, k=k: arrive(part, k))
+                state_send(step + 1, way)
+
+    state_send(1, 0)
+    state_send(1, 1)
+    send(s2.at[z], s2.at[z], k_far_state, z_four, z < 4)
+
+    diagonal([x])
+    slot(2, 0)
+    slot(2, 1)
+    for n in range(1, NX):
+        arrive(qs.at[x_at(NX - n)], k_q[n])
+    diagonal([x_at(n) for n in range(1, NX)])
+    slot(2, 2)
+    attend(1, 0)
+    slot(2, 3)
+    attend(1, 1)
+    state_step(1)
+    slot(3, 0)
+    slot(3, 1)
+    attend(2, 0)
+    slot(3, 2)
+    slot(3, 3)
+    attend(2, 1)
+    state_step(2)
+    attend(3, 0)
+    slot(4, 0)
+    attend(3, 1)
+    slot(4, 1)
+
+    k_o = [site() for _ in range(NX)]
+    k_l = [site() for _ in range(NX)]
+    row8 = iota((8, 128), 0)
+    for pair in ((2, 1), (3, 0)):
+        some = [x_at(n) for n in pair]
+        pl.when(z >= 4)(lambda some=some: update(origin(4, 0), some))
+        for n, j in zip(pair, some):
+            mass = oacc[j][:, HEAD:]
+            op[j] = (oacc[j][:, 0:HEAD] / mass).astype(BF16)
+            if n:
+                send(op.at[j], ob.at[x], k_o[n], (z, j, y, c))
+            height = top[j] + jnp.log(mass)
+            first_row, second_row = row_of(height[0:128]), row_of(height[128:256])
+            lp[j] = jnp.where(row8 == 0, first_row, jnp.where(row8 == 1, second_row, 0.0))
+            if n:
+                send(lp.at[j], lb.at[x], k_l[n], (z, j, y, c))
+
+    state_step(3)
+    far_state = s2.at[lax.rem(z + 4, NZ)]
+    pl.when(z >= 4)(lambda: arrive(far_state, k_far_state))
 
     def earlier(n, state):
         values_n, total_n = unpack(s2.at[n])
@@ -452,27 +534,6 @@
     k_s3 = [site() for _ in range(NX)]
     for n in range(1, NX):
         send(s3s.at[x_at(n)], s3.at[x], k_s3[n], (z, x_at(n), y, c))
-
-    ring(4)
-    attend_both(3)
-    attend(lax.rem(z + 4, NZ))
-
-    def close(j, _):
-        mass = oacc[j][:, HEAD:]
-        op[j] = (oacc[j][:, 0:HEAD] / mass).astype(BF16)
-        height = top[j] + jnp.log(mass)
-        first_row, second_row = row_of(height[0:128]), row_of(height[128:256])
-        row8 = iota((8, 128), 0)
-        lp[j] = jnp.where(row8 == 0, first_row, jnp.where(row8 == 1, second_row, 0.0))
-
-    lax.fori_loop(0, NX, close, None)
-    k_o = [site() for _ in range(NX)]
-    k_l = [site() for _ in range(NX)]
-    for n in range(1, NX):
-        dev = (z, x_at(n), y, c)
-        send(op.at[x_at(n)], ob.at[x], k_o[n], dev)
-        send(lp.at[x_at(n)], lb.at[x], k_l[n], dev)
-
     for n in range(1, NX):
         arrive(s3.at[x_at(NX - n)], k_s3[n])
     s3[x] = s3s[x]
@@ -482,10 +543,9 @@
     heads[:, pl.ds(HEAD, VAL)] = (lin_raw * lax.rsqrt(mean + EPS) * lin_gain[...]).astype(BF16)
 
     for n in range(1, NX):
-        arrive(ob.at[x_at(NX - n)], k_o[n])
         arrive(lb.at[x_at(NX - n)], k_l[n])
+    lb[x] = lp[x]
     ob[x] = op[x]
-    lb[x] = lp[x]
     heights = [lb[n] for n in range(NX)]
     peak = jnp.maximum(jnp.maximum(heights[0], heights[1]), jnp.maximum(heights[2], heights[3]))
     shares = [jnp.exp(h - peak) for h in heights]
@@ -494,14 +554,22 @@
     for n in range(2):
         rows = pl.ds(n * 128, 128)
         log_total[:, rows] = summit[n : n + 1, :]
-        mix = jnp.zeros((128, HEAD), F32)
         for m in range(NX):
-            share = column_of((shares[m] / mass)[n : n + 1, :])
-            mix = mix + share * ob[m, rows, :].astype(F32)
-        heads[rows, pl.ds(0, HEAD)] = mix.astype(BF16)
+            share[m, rows, :] = jnp.broadcast_to(
+                column_of((shares[m] / mass)[n : n + 1, :]), (128, HEAD)
+            )
+    for n in range(1, NX):
+        arrive(ob.at[x_at(NX - n)], k_o[n])
+    mix = share[0] * ob[0].astype(F32)
+    for m in range(1, NX):
+        mix = mix + share[m] * ob[m].astype(F32)
+    heads[:, pl.ds(0, HEAD)] = mix.astype(BF16)
 
     for item in outs:
         item.wait()
+    def landing(n, m):
+        return fin.at[m, :, pl.ds(n * COLS, COLS)]
+
     k_pair = [site() for _ in range(COL_CHUNKS)]
     k_raw = [site() for _ in range(COL_CHUNKS)]
     k_fin = [[site() for _ in range(2)] for _ in range(COL_CHUNKS)]
@@ -518,22 +586,21 @@
     def spread(n):
         arrive(pr.at[n], k_pair[n])
         cb[n] = (pb[n, c].astype(F32) + pr[n].astype(F32)).astype(BF16)
+        own_part[:, pl.ds(n * COLS, COLS)] = cb[n, y]
         near, far = (down, up) if n < col_half else (up, down)
         y_near = ym if n < col_half else yp
         send(cb.at[n, yo], raw.at[n], k_raw[n], far)
-        send(cb.at[n, y_near], fin.at[n, 1], k_fin[n][1], near)
+        send(cb.at[n, y_near], landing(n, 1), k_fin[n][1], near)
 
     def relay(n):
         arrive(raw.at[n], k_raw[n])
         far, y_far = (up, yp) if n < col_half else (down, ym)
         raws[n] = (cb[n, y_far].astype(F32) + raw[n].astype(F32)).astype(BF16)
-        send(raws.at[n], fin.at[n, 0], k_fin[n][0], far)
+        send(raws.at[n], landing(n, 0), k_fin[n][0], far)
 
     def finish(n):
         for m in range(2):
-            arrive(fin.at[n, m], k_fin[n][m])
-        done = cb[n, y].astype(F32) + fin[n, 0].astype(F32) + fin[n, 1].astype(F32)
-        mixed[:, pl.ds(n * COLS, COLS)] = done.astype(BF16)
+            arrive(landing(n, m), k_fin[n][m])
 
     for i in range(COL_CHUNKS + 1):
         if i < COL_CHUNKS:
@@ -559,7 +626,7 @@
 SCRATCH = [
     vmem((NY * NC, TOK, FEAT), BF16),
     vmem((D, 1024), BF16),
-    vmem((D, 16), BF16),
+    vmem((16, D), BF16),
     vmem((HEAD + VAL, D), BF16),
     vmem((TOK, 1024), F32),
     vmem((TOK, 128), F32),
@@ -572,6 +639,7 @@
     vmem((NX, 8, 128), F32),
     vmem((NX, TOK, HEAD), BF16),
     vmem((NX, 8, 128), F32),
+    vmem((NX, TOK, HEAD), F32),
     vmem((TOK, 128), F32),
     vmem((TOK, VAL), F32),
     vmem((TOK, 128), BF16),
@@ -586,7 +654,11 @@
     vmem((COL_CHUNKS, NY, 32, COLS), BF16),
     vmem((COL_CHUNKS, 32, COLS), BF16),
     vmem((COL_CHUNKS, 32, COLS), BF16),
-    vmem((COL_CHUNKS, 2, 32, COLS), BF16),
+    vmem((1, D), F32),
+    vmem((1, NZ * NX * TOK), F32),
+    vmem((16, HEAD), BF16),
+    vmem((1, HEAD), F32),
+    vmem((1, VAL), F32),
     pltpu.SemaphoreType.DMA((N_SEM,)),
     pltpu.SemaphoreType.DMA((N_SEM,)),
     pltpu.SemaphoreType.DMA((N_LOC,)),
@@ -612,16 +684,16 @@
 ):
     here = pl.BlockSpec(memory_space=pltpu.VMEM)
     far = pl.BlockSpec(memory_space=pl.ANY)
-    specs = [far, here, far, far, far, here, far, far, far, far, here, here, here, far, far]
-    return pl.pallas_call(
+    own_part, fin, log_total = pl.pallas_call(
         kernel,
         name="layer",
         out_shape=(
             jax.ShapeDtypeStruct((32, D), BF16),
+            jax.ShapeDtypeStruct((2, 32, D), BF16),
             jax.ShapeDtypeStruct((1, TOK), F32),
         ),
-        in_specs=specs,
-        out_specs=(here, here),
+        in_specs=[far] * 15,
+        out_specs=(here, here, here),
         scratch_shapes=SCRATCH,
         compiler_params=pltpu.CompilerParams(
             collective_id=0, has_side_effects=True, vmem_limit_bytes=60 * 1024 * 1024
@@ -636,13 +708,15 @@
         lin_query,
         lin_key,
         lin_value,
-        decay_down,
+        decay_down.T,
         decay_up,
         decay_bias.reshape(1, HEAD),
         lin_gain.reshape(1, VAL),
         fox_out,
         lin_out,
     )
+    mixed = own_part.astype(F32) + fin[0].astype(F32) + fin[1].astype(F32)
+    return mixed.astype(BF16), log_total
 
 
 def solution(mesh):

time: 74.5 us -> 60 us (0.81)
  Pallas kernels: 68.6 us -> 55.7 us
  local copies, waits for them, and re-layouts: 5.1 us -> 1.22 us
  other arithmetic: 0 us -> 1.91 us
    pallas_call x1, Pallas kernels: 68.6 us -> 55.7 us  [local(): pl.pallas_call(kernel, name='layer', out_shape=(jax.ShapeDtypeStruct((32,...]
    unnamed x3 -> x1, local copies, waits for them, and re-layouts: 5.1 us -> 1.22 us
    convert_element_type x0 -> x1, other arithmetic: none -> 1.91 us  [local(): return (mixed.astype(BF16), log_total)]
where the time goes in v2:
time: 60 us; the launch traced here: 59.5 us
  Pallas kernels  55.7 us (93%)
  other arithmetic  1.91 us (3%)
  local copies, waits for them, and re-layouts  1.22 us (2%)
  between operations  0.65 us (1%)
    pallas_call x1, Pallas kernels, local(): pl.pallas_call(kernel, name='layer', out_shape=(jax.ShapeDtypeStruct((32,...  55.7 us
    convert_element_type x1, other arithmetic, local(): return (mixed.astype(BF16), log_total)  1.91 us
    unnamed x1, local copies, waits for them, and re-layouts  1.22 us

profile of v2, /device:TPU:224, one launch (start us, length us, event | category | flops | bytes accessed | tf_op | source)
XLA Modules:
  0.0 59.5 jit_solution(13249362322265578207)
XLA Ops:
  0.6 55.7 %layer.1 = (bf16[32,4096]{1,0:T(8,128)(2,1)}, bf16[2,32,4096]{2,1,0:T(8,128)(2,1)}, f32[1,256]{1,0:T(1,128)}) custom-call(bf16[256,512]{1,0:T(8,128)(2,1)} %tokens.1, f32[1,4096]{1,0:T(1,128)} %bitcast.11, bf16[4096,128]{1,0:T(8,128)(2,1)} %fox_query.1, bf16[4096,128]{1,0:T(8,128)(2,1)} %fox_key.1, bf16[4096,128]{1,0:T(8,128)(2,1)} %fox_value.1, ...), custom_call_target="tpu_custom_call" | custom-call | tf_op jit(solution)/shard_map/layer/pallas_call | solution.py:687
  56.3 1.9 %fusion = bf16[32,4096]{1,0:T(8,128)(2,1)} fusion(bf16[32,4096]{1,0:T(8,128)(2,1)} %get-tuple-element.5, bf16[2,32,4096]{2,1,0:T(8,128)(2,1)} %get-tuple-element.6), kind=kLoop, calls=%fused_computation.1 | loop fusion | flops 786432 | bytes 1048576 | tf_op jit(solution)/shard_map/convert_element_type | solution.py:719
  58.2 1.2 %copy.18 = f32[1,256]{1,0:T(1,128)} copy(f32[1,256]{1,0:T(1,128)} %get-tuple-element.11) | data formatting | bytes 2048

commit v3 on v2

--- a/solution.py
+++ b/solution.py
@@ -28,6 +28,7 @@
 COL_CHUNKS = 8
 COLS = D // COL_CHUNKS
 N_SEM = 160
+GROUP_DOWN, GROUP_OWN, GROUP_UP = 0, 1, 2
 N_LOC = 16
 
 
@@ -100,6 +101,7 @@
     op,
     lp,
     share,
+    lh,
     lcum,
     lout,
     qext,
@@ -109,9 +111,8 @@
     s3s,
     s3,
     heads,
-    pb,
-    pr,
     cb,
+    far_rows,
     raw,
     raws,
     norm_gain,
@@ -187,7 +188,7 @@
         item.start()
 
     partners = [sib, up, down]
-    partners += [(z, lax.rem(x + n, NX), y, c) for n in range(1, NX)]
+    partners += [(z, lax.rem(x + n, NX), y, core) for n in range(1, NX) for core in (c, other)]
     z_four = (lax.rem(z + 4, NZ), x, y, c)
     partners += [z_up, z_down, z_four]
     barrier = pltpu.get_barrier_semaphore()
@@ -228,12 +229,14 @@
     acc[...] = jnp.zeros_like(acc)
     ssq[...] = jnp.zeros_like(ssq)
 
-    def project(block):
+    def project(block, start=0, width=1024):
         xb = xg[block].astype(F32)
-        ssq[...] += jnp.sum(xb * xb, axis=1, keepdims=True)
+        if start == 0:
+            ssq[...] += jnp.sum(xb * xb, axis=1, keepdims=True)
         rows = pl.multiple_of(block * FEAT, FEAT)
         gain = norm_gain[:, pl.ds(rows, FEAT)]
-        acc[...] += mm((xb * gain).astype(BF16), w[pl.ds(rows, FEAT), :])
+        cols = pl.ds(start, width)
+        acc[:, cols] += mm((xb * gain).astype(BF16), w[pl.ds(rows, FEAT), cols])
 
     project(own)
     for n in range(half):
@@ -269,7 +272,7 @@
     project(b_o)
     for n in range(CHUNKS):
         arrive(piece(s_o, n), k_relay[2][n])
-    project(s_o)
+    project(s_o, 0, 512)
 
     norm = lax.rsqrt(ssq[:, 0:1] * (1.0 / D) + EPS)
 
@@ -282,7 +285,7 @@
     kv_half = KV_CHUNKS // 2
 
     def reach(n):
-        return (4, 3) if n < kv_half else (3, 4)
+        return (4, 3) if n < KV_CHUNKS - 1 else (3, 4)
 
     k_kv = {}
     for step in range(1, 5):
@@ -331,6 +334,12 @@
 
     def x_at(n):
         return lax.rem(x + n, NX)
+
+    project(s_o, 512, 512)
+
+    k_wo = [site(), site()]
+    send(fox_out, wo.at[pl.ds(HEAD + VAL, HEAD), :], k_wo[0], sib)
+    send(lin_out, wo.at[pl.ds(2 * HEAD + VAL, VAL), :], k_wo[1], sib)
 
     lk = result(512, 128).astype(BF16).astype(F32)
     lv = result(640, 256).astype(BF16)
@@ -446,8 +455,6 @@
 
     slot(1, 0)
     slot(1, 1)
-    slot(1, 2)
-    slot(1, 3)
 
     for n in range(1, NX):
         arrive(s1.at[x_at(NX - n)], k_s1[n])
@@ -478,9 +485,12 @@
     state_send(1, 1)
     send(s2.at[z], s2.at[z], k_far_state, z_four, z < 4)
 
+    slot(1, 2)
+    slot(1, 3)
     diagonal([x])
     slot(2, 0)
     slot(2, 1)
+    state_step(1)
     for n in range(1, NX):
         arrive(qs.at[x_at(NX - n)], k_q[n])
     diagonal([x_at(n) for n in range(1, NX)])
@@ -488,35 +498,14 @@
     attend(1, 0)
     slot(2, 3)
     attend(1, 1)
-    state_step(1)
+    attend(2, 0)
+    state_step(2)
     slot(3, 0)
     slot(3, 1)
-    attend(2, 0)
+    attend(2, 1)
     slot(3, 2)
     slot(3, 3)
-    attend(2, 1)
-    state_step(2)
     attend(3, 0)
-    slot(4, 0)
-    attend(3, 1)
-    slot(4, 1)
-
-    k_o = [site() for _ in range(NX)]
-    k_l = [site() for _ in range(NX)]
-    row8 = iota((8, 128), 0)
-    for pair in ((2, 1), (3, 0)):
-        some = [x_at(n) for n in pair]
-        pl.when(z >= 4)(lambda some=some: update(origin(4, 0), some))
-        for n, j in zip(pair, some):
-            mass = oacc[j][:, HEAD:]
-            op[j] = (oacc[j][:, 0:HEAD] / mass).astype(BF16)
-            if n:
-                send(op.at[j], ob.at[x], k_o[n], (z, j, y, c))
-            height = top[j] + jnp.log(mass)
-            first_row, second_row = row_of(height[0:128]), row_of(height[128:256])
-            lp[j] = jnp.where(row8 == 0, first_row, jnp.where(row8 == 1, second_row, 0.0))
-            if n:
-                send(lp.at[j], lb.at[x], k_l[n], (z, j, y, c))
 
     state_step(3)
     far_state = s2.at[lax.rem(z + 4, NZ)]
@@ -534,79 +523,149 @@
     k_s3 = [site() for _ in range(NX)]
     for n in range(1, NX):
         send(s3s.at[x_at(n)], s3.at[x], k_s3[n], (z, x_at(n), y, c))
+
+    slot(4, 0)
+    slot(4, 1)
+    attend(3, 1)
+    slot(4, 2)
+    slot(4, 3)
+
+    k_o = [[site(), site()] for _ in range(NX)]
+    k_rest = [[site(), site()] for _ in range(NX)]
+    rest = pl.ds(1, NY - 1)
+    k_l = [[site(), site()] for _ in range(NX)]
+    row8 = iota((8, 128), 0)
+    cores = (c, other)
+
+    def of_core(value, core):
+        parts = value.reshape(NY, NC, 32, value.shape[1])
+        return parts[:, core].reshape(TOK // 2, value.shape[1])
+
+    def keep(ref, value):
+        for n in range(NY):
+            ref[lax.rem(n + NY - yo, NY)] = value[n * 32 : (n + 1) * 32]
+
+
+    for pair in ((2, 1), (3, 0)):
+        some = [x_at(n) for n in pair]
+        pl.when(z >= 4)(lambda some=some: update(origin(4, 0), some))
+        for n, j in zip(pair, some):
+            mass = oacc[j][:, HEAD:]
+            height = top[j] + jnp.log(mass)
+            row = [row_of(of_core(height, core)) for core in range(NC)]
+            lp[j] = jnp.where(row8 == 0, row[0], jnp.where(row8 == 1, row[1], 0.0))
+            result_j = (oacc[j][:, 0:HEAD] / mass).astype(BF16)
+            for core in range(NC):
+                keep(op.at[j, core], of_core(result_j, core))
+            for h in range(2):
+                if n or h:
+                    dev = (z, j, y, cores[h])
+                    send(lp.at[j], lb.at[h, x], k_l[n][h], dev)
+                    send(op.at[j, cores[h], 0], ob.at[h, x, 0], k_o[n][h], dev)
+    for n in (2, 1, 3, 0):
+        for h in range(2):
+            if n or h:
+                dev = (z, x_at(n), y, cores[h])
+                part = op.at[x_at(n), cores[h], rest]
+                send(part, ob.at[h, x, rest], k_rest[n][h], dev)
+
     for n in range(1, NX):
         arrive(s3.at[x_at(NX - n)], k_s3[n])
     s3[x] = s3s[x]
     whole = jnp.concatenate([s3[n] for n in range(NX)], axis=0)
     lin_raw = lout[...] + nt(qext[...], whole)
     mean = jnp.mean(lin_raw * lin_raw, axis=1, keepdims=True)
-    heads[:, pl.ds(HEAD, VAL)] = (lin_raw * lax.rsqrt(mean + EPS) * lin_gain[...]).astype(BF16)
-
-    for n in range(1, NX):
-        arrive(lb.at[x_at(NX - n)], k_l[n])
-    lb[x] = lp[x]
-    ob[x] = op[x]
-    heights = [lb[n] for n in range(NX)]
-    peak = jnp.maximum(jnp.maximum(heights[0], heights[1]), jnp.maximum(heights[2], heights[3]))
-    shares = [jnp.exp(h - peak) for h in heights]
-    mass = shares[0] + shares[1] + shares[2] + shares[3]
-    summit = peak + jnp.log(mass)
-    for n in range(2):
-        rows = pl.ds(n * 128, 128)
-        log_total[:, rows] = summit[n : n + 1, :]
+    lin_done = (lin_raw * lax.rsqrt(mean + EPS) * lin_gain[...]).astype(BF16)
+    for core in range(NC):
+        keep(lh.at[core], of_core(lin_done, core))
+    k_lh = site()
+    lin_there = heads.at[:, :, pl.ds(2 * HEAD + VAL, VAL)]
+    send(lh.at[other], lin_there, k_lh, sib)
+    heads[:, :, pl.ds(HEAD, VAL)] = lh[c]
+
+    for n in range(NX):
+        for h in range(2):
+            if n or h:
+                arrive(lb.at[h, x_at(NX - n)], k_l[n][h])
+    lb[0, x] = lp[x]
+    ob[0, x] = op[x, c]
+    summit = None
+    for h in range(2):
+        heights = [lb[h, n] for n in range(NX)]
+        peak = jnp.maximum(
+            jnp.maximum(heights[0], heights[1]), jnp.maximum(heights[2], heights[3])
+        )
+        shares = [jnp.exp(height - peak) for height in heights]
+        mass = shares[0] + shares[1] + shares[2] + shares[3]
+        if h == 0:
+            summit = peak + jnp.log(mass)
         for m in range(NX):
-            share[m, rows, :] = jnp.broadcast_to(
-                column_of((shares[m] / mass)[n : n + 1, :]), (128, HEAD)
-            )
-    for n in range(1, NX):
-        arrive(ob.at[x_at(NX - n)], k_o[n])
-    mix = share[0] * ob[0].astype(F32)
-    for m in range(1, NX):
-        mix = mix + share[m] * ob[m].astype(F32)
-    heads[:, pl.ds(0, HEAD)] = mix.astype(BF16)
-
+            even = (shares[m] / mass)[0:2, :]
+            mine_row = jnp.where(c == 0, even[0:1, :], even[1:2, :])
+            keep(share.at[h, m], jnp.broadcast_to(column_of(mine_row), (128, HEAD)))
+    parts = []
+    for n in range(NY):
+        for core in range(NC):
+            parts.append(summit[core : core + 1, n * 32 : (n + 1) * 32])
+    log_total[...] = jnp.concatenate(parts, axis=1)
     for item in outs:
         item.wait()
+    arrive(wo.at[pl.ds(HEAD + VAL, HEAD), :], k_wo[0])
+    arrive(wo.at[pl.ds(2 * HEAD + VAL, VAL), :], k_wo[1])
+    arrive(lin_there, k_lh)
     def landing(n, m):
         return fin.at[m, :, pl.ds(n * COLS, COLS)]
 
-    k_pair = [site() for _ in range(COL_CHUNKS)]
     k_raw = [site() for _ in range(COL_CHUNKS)]
     k_fin = [[site() for _ in range(2)] for _ in range(COL_CHUNKS)]
     col_half = COL_CHUNKS // 2
     order = [n + half_n for n in range(col_half) for half_n in (0, col_half)]
 
-    def produce(n):
-        part = mm(heads[...], wo[:, pl.ds(n * COLS, COLS)]).astype(BF16)
-        part = part.reshape(NY, NC, 32, COLS)
-        for m in range(NC):
-            pb[n, m] = part[:, m]
-        send(pb.at[n, other], pr.at[n], k_pair[n], sib)
-
-    def spread(n):
-        arrive(pr.at[n], k_pair[n])
-        cb[n] = (pb[n, c].astype(F32) + pr[n].astype(F32)).astype(BF16)
-        own_part[:, pl.ds(n * COLS, COLS)] = cb[n, y]
-        near, far = (down, up) if n < col_half else (up, down)
-        y_near = ym if n < col_half else yp
-        send(cb.at[n, yo], raw.at[n], k_raw[n], far)
-        send(cb.at[n, y_near], landing(n, 1), k_fin[n][1], near)
+    def ways(n):
+        return (up, GROUP_UP, down, GROUP_DOWN) if n < col_half else (down, GROUP_DOWN, up, GROUP_UP)
+
+    def wait_parts(keys, groups):
+        for n in range(NX):
+            for h in range(2):
+                if n or h:
+                    arrive(ob.at[h, x_at(NX - n), groups], keys[n][h])
+
+    def mix(groups):
+        for h in range(2):
+            total = share[h, 0, groups] * ob[h, 0, groups].astype(F32)
+            for m in range(1, NX):
+                total = total + share[h, m, groups] * ob[h, m, groups].astype(F32)
+            heads[groups, :, pl.ds(h * (HEAD + VAL), HEAD)] = total.astype(BF16)
+
+    wait_parts(k_o, 0)
+    mix(0)
+    for n in order:
+        far_rows[n] = mm(heads[0], wo[:, pl.ds(n * COLS, COLS)]).astype(BF16)
+        send(far_rows.at[n], raw.at[n], k_raw[n], ways(n)[0])
+    wait_parts(k_rest, rest)
+    mix(rest)
+
+    def direct(n):
+        left = heads[rest].reshape(96, 2 * (HEAD + VAL))
+        part = mm(left, wo[:, pl.ds(n * COLS, COLS)])
+        cb[n] = part.astype(BF16).reshape(NY - 1, 32, COLS)
+        near, group = ways(n)[2:]
+        send(cb.at[n, group], landing(n, 1), k_fin[n][1], near)
 
     def relay(n):
         arrive(raw.at[n], k_raw[n])
-        far, y_far = (up, yp) if n < col_half else (down, ym)
-        raws[n] = (cb[n, y_far].astype(F32) + raw[n].astype(F32)).astype(BF16)
+        far, group = ways(n)[:2]
+        raws[n] = (cb[n, group].astype(F32) + raw[n].astype(F32)).astype(BF16)
         send(raws.at[n], landing(n, 0), k_fin[n][0], far)
 
     def finish(n):
         for m in range(2):
             arrive(landing(n, m), k_fin[n][m])
 
-    for i in range(COL_CHUNKS + 1):
-        if i < COL_CHUNKS:
-            produce(order[i])
-        if i:
-            spread(order[i - 1])
+    for n in order:
+        direct(n)
+    for n in range(COL_CHUNKS):
+        own_part[:, pl.ds(n * COLS, COLS)] = cb[n, GROUP_OWN]
     for n in order:
         relay(n)
     for n in order:
@@ -619,6 +678,12 @@
             pl.when(when)(lambda a=(src, dst, k, dev): copy(*a).wait_send())
 
 
+def finish_kernel(own_part, fin, log_in, mixed, log_out):
+    total = own_part[...].astype(F32) + fin[0].astype(F32) + fin[1].astype(F32)
+    mixed[...] = total.astype(BF16)
+    log_out[...] = log_in[...]
+
+
 def vmem(shape, dtype):
     return pltpu.VMEM(shape, dtype)
 
@@ -627,7 +692,7 @@
     vmem((NY * NC, TOK, FEAT), BF16),
     vmem((D, 1024), BF16),
     vmem((16, D), BF16),
-    vmem((HEAD + VAL, D), BF16),
+    vmem((2 * (HEAD + VAL), D), BF16),
     vmem((TOK, 1024), F32),
     vmem((TOK, 128), F32),
     vmem((NX, TOK, HEAD), BF16),
@@ -635,11 +700,12 @@
     vmem((NX, TOK, 128), F32),
     vmem((NX, TOK, 128), F32),
     vmem((NX, TOK, 2 * HEAD), F32),
-    vmem((NX, TOK, HEAD), BF16),
+    vmem((2, NX, NY, 32, HEAD), BF16),
+    vmem((2, NX, 8, 128), F32),
+    vmem((NX, NC, NY, 32, HEAD), BF16),
     vmem((NX, 8, 128), F32),
-    vmem((NX, TOK, HEAD), BF16),
-    vmem((NX, 8, 128), F32),
-    vmem((NX, TOK, HEAD), F32),
+    vmem((2, NX, NY, 32, HEAD), F32),
+    vmem((NC, NY, 32, VAL), BF16),
     vmem((TOK, 128), F32),
     vmem((TOK, VAL), F32),
     vmem((TOK, 128), BF16),
@@ -648,10 +714,9 @@
     vmem((NZ, VAL // NX + 16, 128), BF16),
     vmem((NX, VAL // NX, 128), BF16),
     vmem((NX, VAL // NX, 128), BF16),
-    vmem((TOK, HEAD + VAL), BF16),
-    vmem((COL_CHUNKS, NC, NY, 32, COLS), BF16),
-    vmem((COL_CHUNKS, NY, 32, COLS), BF16),
-    vmem((COL_CHUNKS, NY, 32, COLS), BF16),
+    vmem((NY, 32, 2 * (HEAD + VAL)), BF16),
+    vmem((COL_CHUNKS, NY - 1, 32, COLS), BF16),
+    vmem((COL_CHUNKS, 32, COLS), BF16),
     vmem((COL_CHUNKS, 32, COLS), BF16),
     vmem((COL_CHUNKS, 32, COLS), BF16),
     vmem((1, D), F32),
@@ -715,8 +780,16 @@
         fox_out,
         lin_out,
     )
-    mixed = own_part.astype(F32) + fin[0].astype(F32) + fin[1].astype(F32)
-    return mixed.astype(BF16), log_total
+    return pl.pallas_call(
+        finish_kernel,
+        name="finish",
+        out_shape=(
+            jax.ShapeDtypeStruct((32, D), BF16),
+            jax.ShapeDtypeStruct((1, TOK), F32),
+        ),
+        in_specs=[here] * 3,
+        out_specs=(here, here),
+    )(own_part, fin, log_total)
 
 
 def solution(mesh):

time: 60 us -> 56.2 us (0.937)
  the two profiles are of different devices: /device:TPU:224 before, /device:TPU:166 now
where the time goes in v3:
time: 56.2 us; the launch traced here: 56.1 us
  Pallas kernels  55.4 us (99%)
  between operations  0.64 us (1%)
    pallas_call x1, Pallas kernels, local(): pl.pallas_call(kernel, name='layer', out_shape=(jax.ShapeDtypeStruct((32,...  53.5 us
    pallas_call x1, Pallas kernels, local(): pl.pallas_call(finish_kernel, name='finish', out_shape=(jax.ShapeDtypeStr...  1.91 us

profile of v3, /device:TPU:166, one launch (start us, length us, event | category | flops | bytes accessed | tf_op | source)
XLA Modules:
  0.0 56.1 jit_solution(15871779951100142864)
XLA Ops:
  0.6 53.5 %layer.1 = (bf16[32,4096]{1,0:T(8,128)(2,1)}, bf16[2,32,4096]{2,1,0:T(8,128)(2,1)}, f32[1,256]{1,0:T(1,128)}) custom-call(bf16[256,512]{1,0:T(8,128)(2,1)} %tokens.1, f32[1,4096]{1,0:T(1,128)} %bitcast.5, bf16[4096,128]{1,0:T(8,128)(2,1)} %fox_query.1, bf16[4096,128]{1,0:T(8,128)(2,1)} %fox_key.1, bf16[4096,128]{1,0:T(8,128)(2,1)} %fox_value.1, ...), custom_call_target="tpu_custom_call" | custom-call | tf_op jit(solution)/shard_map/layer/pallas_call | solution.py:752
  54.2 1.9 %finish.1 = (bf16[32,4096]{1,0:T(8,128)(2,1)}, f32[1,256]{1,0:T(1,128)}) custom-call(bf16[32,4096]{1,0:T(8,128)(2,1)} %get-tuple-element.5.own_part, bf16[2,32,4096]{2,1,0:T(8,128)(2,1)} %get-tuple-element.6.fin, f32[1,256]{1,0:T(1,128)} %get-tuple-element.7.log_in), custom_call_target="tpu_custom_call" | custom-call | tf_op jit(solution)/shard_map/finish/pallas_call | solution.py:783

commit v4 on v3

--- a/solution.py
+++ b/solution.py
@@ -82,8 +82,7 @@
     lin_gain_far,
     fox_out,
     lin_out,
-    own_part,
-    fin,
+    mixed,
     log_total,
     xg,
     w,
@@ -115,6 +114,7 @@
     far_rows,
     raw,
     raws,
+    fin,
     norm_gain,
     cum_gate,
     decay_up,
@@ -163,6 +163,13 @@
     own = y * 2 + c
     first = pltpu.make_async_copy(tokens, xg.at[own], ls.at[0])
     first.start()
+    partners = [sib, up, down]
+    partners += [(z, lax.rem(x + n, NX), y, core) for n in range(1, NX) for core in (c, other)]
+    z_four = (lax.rem(z + 4, NZ), x, y, c)
+    partners += [z_up, z_down, z_four]
+    barrier = pltpu.get_barrier_semaphore()
+    for dev in partners:
+        pl.semaphore_signal(barrier, inc=1, device_id=dev, device_id_type=MESH)
     weights = []
     column = 0
     for n, ref in enumerate((fox_query, fox_key, fox_value, lin_query, lin_key, lin_value)):
@@ -184,16 +191,7 @@
         pltpu.make_async_copy(fox_out, wo.at[pl.ds(0, HEAD), :], ls.at[8]),
         pltpu.make_async_copy(lin_out, wo.at[pl.ds(HEAD, VAL), :], ls.at[9]),
     ]
-    for item in outs:
-        item.start()
-
-    partners = [sib, up, down]
-    partners += [(z, lax.rem(x + n, NX), y, core) for n in range(1, NX) for core in (c, other)]
-    z_four = (lax.rem(z + 4, NZ), x, y, c)
-    partners += [z_up, z_down, z_four]
-    barrier = pltpu.get_barrier_semaphore()
-    for dev in partners:
-        pl.semaphore_signal(barrier, inc=1, device_id=dev, device_id_type=MESH)
+
     pl.semaphore_wait(barrier, len(partners))
 
     first.wait()
@@ -337,6 +335,8 @@
 
     project(s_o, 512, 512)
 
+    for item in outs:
+        item.start()
     k_wo = [site(), site()]
     send(fox_out, wo.at[pl.ds(HEAD + VAL, HEAD), :], k_wo[0], sib)
     send(lin_out, wo.at[pl.ds(2 * HEAD + VAL, VAL), :], k_wo[1], sib)
@@ -524,9 +524,9 @@
     for n in range(1, NX):
         send(s3s.at[x_at(n)], s3.at[x], k_s3[n], (z, x_at(n), y, c))
 
+    attend(3, 1)
     slot(4, 0)
     slot(4, 1)
-    attend(3, 1)
     slot(4, 2)
     slot(4, 3)
 
@@ -546,7 +546,7 @@
             ref[lax.rem(n + NY - yo, NY)] = value[n * 32 : (n + 1) * 32]
 
 
-    for pair in ((2, 1), (3, 0)):
+    for pair in ((2, 1, 3, 0),):
         some = [x_at(n) for n in pair]
         pl.when(z >= 4)(lambda some=some: update(origin(4, 0), some))
         for n, j in zip(pair, some):
@@ -590,6 +590,7 @@
     lb[0, x] = lp[x]
     ob[0, x] = op[x, c]
     summit = None
+    share_rows = {}
     for h in range(2):
         heights = [lb[h, n] for n in range(NX)]
         peak = jnp.maximum(
@@ -600,14 +601,18 @@
         if h == 0:
             summit = peak + jnp.log(mass)
         for m in range(NX):
-            even = (shares[m] / mass)[0:2, :]
-            mine_row = jnp.where(c == 0, even[0:1, :], even[1:2, :])
-            keep(share.at[h, m], jnp.broadcast_to(column_of(mine_row), (128, HEAD)))
-    parts = []
-    for n in range(NY):
-        for core in range(NC):
-            parts.append(summit[core : core + 1, n * 32 : (n + 1) * 32])
-    log_total[...] = jnp.concatenate(parts, axis=1)
+            even = shares[m] / mass
+            share_rows[h, m] = jnp.where(c == 0, even[0:1, :], even[1:2, :])
+
+    def columns(group):
+        place = iota((32, 128), 0) + lax.rem(yo + group, NY) * 32
+        for h in range(2):
+            for m in range(NX):
+                picked = jnp.where(iota((32, 128), 1) == place, share_rows[h, m], 0.0)
+                column = jnp.sum(picked, axis=1, keepdims=True)
+                share[h, m, group] = jnp.broadcast_to(column, (32, HEAD))
+
+    columns(0)
     for item in outs:
         item.wait()
     arrive(wo.at[pl.ds(HEAD + VAL, HEAD), :], k_wo[0])
@@ -642,6 +647,13 @@
     for n in order:
         far_rows[n] = mm(heads[0], wo[:, pl.ds(n * COLS, COLS)]).astype(BF16)
         send(far_rows.at[n], raw.at[n], k_raw[n], ways(n)[0])
+    parts = []
+    for n in range(NY):
+        for core in range(NC):
+            parts.append(summit[core : core + 1, n * 32 : (n + 1) * 32])
+    log_total[...] = jnp.concatenate(parts, axis=1)
+    for group in range(1, NY):
+        columns(group)
     wait_parts(k_rest, rest)
     mix(rest)
 
@@ -661,11 +673,12 @@
     def finish(n):
         for m in range(2):
             arrive(landing(n, m), k_fin[n][m])
+        cols = pl.ds(n * COLS, COLS)
+        done = cb[n, GROUP_OWN].astype(F32) + fin[0, :, cols].astype(F32)
+        mixed[:, cols] = (done + fin[1, :, cols].astype(F32)).astype(BF16)
 
     for n in order:
         direct(n)
-    for n in range(COL_CHUNKS):
-        own_part[:, pl.ds(n * COLS, COLS)] = cb[n, GROUP_OWN]
     for n in order:
         relay(n)
     for n in order:
@@ -678,9 +691,8 @@
             pl.when(when)(lambda a=(src, dst, k, dev): copy(*a).wait_send())
 
 
-def finish_kernel(own_part, fin, log_in, mixed, log_out):
-    total = own_part[...].astype(F32) + fin[0].astype(F32) + fin[1].astype(F32)
-    mixed[...] = total.astype(BF16)
+def finish_kernel(mixed_in, log_in, mixed_out, log_out):
+    mixed_out[...] = mixed_in[...]
     log_out[...] = log_in[...]
 
 
@@ -719,6 +731,7 @@
     vmem((COL_CHUNKS, 32, COLS), BF16),
     vmem((COL_CHUNKS, 32, COLS), BF16),
     vmem((COL_CHUNKS, 32, COLS), BF16),
+    vmem((2, 32, D), BF16),
     vmem((1, D), F32),
     vmem((1, NZ * NX * TOK), F32),
     vmem((16, HEAD), BF16),
@@ -749,16 +762,15 @@
 ):
     here = pl.BlockSpec(memory_space=pltpu.VMEM)
     far = pl.BlockSpec(memory_space=pl.ANY)
-    own_part, fin, log_total = pl.pallas_call(
+    mixed, log_total = pl.pallas_call(
         kernel,
         name="layer",
         out_shape=(
             jax.ShapeDtypeStruct((32, D), BF16),
-            jax.ShapeDtypeStruct((2, 32, D), BF16),
             jax.ShapeDtypeStruct((1, TOK), F32),
         ),
         in_specs=[far] * 15,
-        out_specs=(here, here, here),
+        out_specs=(here, here),
         scratch_shapes=SCRATCH,
         compiler_params=pltpu.CompilerParams(
             collective_id=0, has_side_effects=True, vmem_limit_bytes=60 * 1024 * 1024
@@ -787,9 +799,9 @@
             jax.ShapeDtypeStruct((32, D), BF16),
             jax.ShapeDtypeStruct((1, TOK), F32),
         ),
-        in_specs=[here] * 3,
+        in_specs=[here] * 2,
         out_specs=(here, here),
-    )(own_part, fin, log_total)
+    )(mixed, log_total)
 
 
 def solution(mesh):

time: 56.2 us -> 55.4 us (0.986)
  the two profiles are of different devices: /device:TPU:166 before, /device:TPU:224 now
where the time goes in v4:
time: 55.4 us; the launch traced here: 54.4 us
  Pallas kernels  53.7 us (97%)
  between operations  0.64 us (1%)
    pallas_call x1, Pallas kernels, local(): pl.pallas_call(kernel, name='layer', out_shape=(jax.ShapeDtypeStruct((32,...  52 us
    pallas_call x1, Pallas kernels, local(): pl.pallas_call(finish_kernel, name='finish', out_shape=(jax.ShapeDtypeStr...  1.68 us

profile of v4, /device:TPU:224, one launch (start us, length us, event | category | flops | bytes accessed | tf_op | source)
XLA Modules:
  0.0 54.4 jit_solution(15813274323678005184)
XLA Ops:
  0.6 52.0 %layer.1 = (bf16[32,4096]{1,0:T(8,128)(2,1)}, f32[1,256]{1,0:T(1,128)}) custom-call(bf16[256,512]{1,0:T(8,128)(2,1)} %tokens.1, f32[1,4096]{1,0:T(1,128)} %bitcast.5, bf16[4096,128]{1,0:T(8,128)(2,1)} %fox_query.1, bf16[4096,128]{1,0:T(8,128)(2,1)} %fox_key.1, bf16[4096,128]{1,0:T(8,128)(2,1)} %fox_value.1, f32[1,8192]{1,0:T(1,128)} %cum_gate_far.1, ...), custom_call_target="tpu_custom_call" | custom-call | tf_op jit(solution)/shard_map/layer/pallas_call | solution.py:765
  52.7 1.7 %finish.1 = (bf16[32,4096]{1,0:T(8,128)(2,1)}, f32[1,256]{1,0:T(1,128)}) custom-call(bf16[32,4096]{1,0:T(8,128)(2,1)} %get-tuple-element.4.mixed_in, f32[1,256]{1,0:T(1,128)} %get-tuple-element.5.log_in), custom_call_target="tpu_custom_call" | custom-call | tf_op jit(solution)/shard_map/finish/pallas_call | solution.py:795

commit v5 on v4

--- a/solution.py
+++ b/solution.py
@@ -335,12 +335,6 @@
 
     project(s_o, 512, 512)
 
-    for item in outs:
-        item.start()
-    k_wo = [site(), site()]
-    send(fox_out, wo.at[pl.ds(HEAD + VAL, HEAD), :], k_wo[0], sib)
-    send(lin_out, wo.at[pl.ds(2 * HEAD + VAL, VAL), :], k_wo[1], sib)
-
     lk = result(512, 128).astype(BF16).astype(F32)
     lv = result(640, 256).astype(BF16)
     low = result(896, 128).astype(BF16)
@@ -498,6 +492,11 @@
     attend(1, 0)
     slot(2, 3)
     attend(1, 1)
+    for item in outs:
+        item.start()
+    k_wo = [site(), site()]
+    send(fox_out, wo.at[pl.ds(HEAD + VAL, HEAD), :], k_wo[0], sib)
+    send(lin_out, wo.at[pl.ds(2 * HEAD + VAL, VAL), :], k_wo[1], sib)
     attend(2, 0)
     state_step(2)
     slot(3, 0)
@@ -505,8 +504,6 @@
     attend(2, 1)
     slot(3, 2)
     slot(3, 3)
-    attend(3, 0)
-
     state_step(3)
     far_state = s2.at[lax.rem(z + 4, NZ)]
     pl.when(z >= 4)(lambda: arrive(far_state, k_far_state))
@@ -524,6 +521,7 @@
     for n in range(1, NX):
         send(s3s.at[x_at(n)], s3.at[x], k_s3[n], (z, x_at(n), y, c))
 
+    attend(3, 0)
     attend(3, 1)
     slot(4, 0)
     slot(4, 1)

time: 55.4 us -> 55.5 us (level)
  no operation moved by 1% of the time
where the time goes in v5:
time: 55.5 us; the launch traced here: 54.6 us
  Pallas kernels  54 us (97%)
  between operations  0.64 us (1%)
    pallas_call x1, Pallas kernels, local(): pl.pallas_call(kernel, name='layer', out_shape=(jax.ShapeDtypeStruct((32,...  52.3 us
    pallas_call x1, Pallas kernels, local(): pl.pallas_call(finish_kernel, name='finish', out_shape=(jax.ShapeDtypeStr...  1.68 us

profile of v5, /device:TPU:224, one launch (start us, length us, event | category | flops | bytes accessed | tf_op | source)
XLA Modules:
  0.0 54.6 jit_solution(16792445692280888229)
XLA Ops:
  0.6 52.3 %layer.1 = (bf16[32,4096]{1,0:T(8,128)(2,1)}, f32[1,256]{1,0:T(1,128)}) custom-call(bf16[256,512]{1,0:T(8,128)(2,1)} %tokens.1, f32[1,4096]{1,0:T(1,128)} %bitcast.5, bf16[4096,128]{1,0:T(8,128)(2,1)} %fox_query.1, bf16[4096,128]{1,0:T(8,128)(2,1)} %fox_key.1, bf16[4096,128]{1,0:T(8,128)(2,1)} %fox_value.1, f32[1,8192]{1,0:T(1,128)} %cum_gate_far.1, ...), custom_call_target="tpu_custom_call" | custom-call | tf_op jit(solution)/shard_map/layer/pallas_call | solution.py:763
  53.0 1.7 %finish.1 = (bf16[32,4096]{1,0:T(8,128)(2,1)}, f32[1,256]{1,0:T(1,128)}) custom-call(bf16[32,4096]{1,0:T(8,128)(2,1)} %get-tuple-element.4.mixed_in, f32[1,256]{1,0:T(1,128)} %get-tuple-element.5.log_in), custom_call_target="tpu_custom_call" | custom-call | tf_op jit(solution)/shard_map/finish/pallas_call | solution.py:793
